TPU v7x, 128 devices: a whole 4x4x4 slice. The times are simulated.
128 devices in a mesh: sp: 16 (over z, x), tp: 8 (over y, core).
Axes of the slice: x: 4, y: 4, z: 4, core: 2. Of those that a mesh axis runs over, the one named last changes fastest.
Arguments:
- tokens: bfloat16 [16384, 2048], P(('sp', 'tp')), may hold values from -6 to 6
- elapsed: float32 [16384], P(('sp', 'tp')), may hold values from 0 to 3, as said below
- norm_gain: float32 [2048], replicated, may hold values from 0.1 to 1.9
- in_weight: bfloat16 [2048, 1024], replicated, may hold values from -0.125 to 0.125
- state_input: bfloat16 [2, 2, 64, 64, 16], replicated, may hold values from -1.5 to 1.5
- state_output: float32 [2, 2, 64, 16, 64], replicated, may hold values from -0.375 to 0.375
- forget_rate: float32 [2, 64, 64], replicated, may hold values from 0 to 1, as said below
- decay_angle: float32 [2, 64, 64], replicated, may hold values from -3.140625 to 3.140625
- skip_gain: float32 [1024], replicated, may hold values from -4 to 4
- glu_weight: bfloat16 [1024, 1024], replicated, may hold values from -0.1875 to 0.1875
- glu_bias: float32 [1024], replicated, may hold values from -4 to 4
- out_weight: bfloat16 [1024, 2048], replicated, may hold values from -0.1875 to 0.1875
- out_gain: float32 [2048], replicated, may hold values from 0.1 to 1.9
Outputs:
- mixed: bfloat16 [16384, 2048], P(('sp', 'tp'))
Inputs may be any that keep to these rules, and one draw needn't show every extreme that they name: `elapsed`: positive time steps. `forget_rate`: positive rates.
All inputs are finite; a program needn't handle non-finite values.
Results may differ from a plain program's by a relative error of at most 0.0067.
Values sent between devices are 32-bit elements; how exact they have to be, the bound alone decides.
A program may use at most 128 MiB of HBM per device.

v0:
```python
import functools
import math

import jax
import jax.numpy as jnp
from jax import lax
from jax.experimental import pallas as pl
from jax.experimental.pallas import tpu as pltpu
from jax.sharding import PartitionSpec as P

F32 = jnp.float32
BF16 = jnp.bfloat16
MESH = pl.DeviceIdType.MESH

ROWS = 128
TILES = 32
SUBS = 8
STEPS = 16
NEAR = 4
EPS = 1e-06
LOG2E = 1.4426950408889634
SIN_C = (4.442883014678955, -7.308241367340088, 3.6062889099121094, -0.845763623714447, 0.10920575261116028)
COS_C = (1.4142135381698608, -6.9788641929626465, 5.73988151550293, -1.8882750272750854, 0.3322518765926361, -0.034502167254686356)
INV_TURN = 1.0 / (2.0 * math.pi)
TURN_HI = math.floor(INV_TURN * 4096.0) / 4096.0
TURN_LO = INV_TURN - TURN_HI


def horner(x, coefficients):
    total = coefficients[-1]
    for c in coefficients[-2::-1]:
        total = total * x + c
    return total


def half_turn_parts(turns):
    part = turns - lax.round(turns, lax.RoundingMethod.TO_NEAREST_EVEN)
    square = part * part
    return part * horner(square, SIN_C), horner(square, COS_C)


def decay_parts(size, turns):
    sine, cosine = half_turn_parts(turns)
    lean = size * sine
    return size - lean * sine, lean * cosine


def times(a_re, a_im, b_re, b_im):
    return a_re * b_re - a_im * b_im, a_re * b_im + a_im * b_re


def kernel(
    tokens_h, elapsed_h, ngain_h, inw_h, sin_h, sout_h, rate_h, angle_h, skip_h, glu_h, gbias_h, outw_h, ogain_h,
    out_ref,
    tokens_v, elapsed_v, ngain_v, inw_v, sin_v, sout_v, rate_v, angle_v, skip_v, glu_v, gbias_v, outw_v, ogain_v,
    normed, acc, drv, resp, bst, cst, proj, dec, tabs, dts, spans, loc, ssum, lead, fade, ent,
    t_own, t_par, t_y, t_x, t_z, s_par, s_y, s_x, s_z, s_fin, s_in,
    dma_sem, t_send, t_recv, d_send, d_recv,
):
    sp = lax.axis_index("sp")
    tp = lax.axis_index("tp")
    zi, xi = sp // NEAR, sp % NEAR
    yi, core = tp // 2, tp % 2
    way = 1 - core

    def partner():
        return {"sp": sp, "tp": yi * 2 + (1 - core)}

    def along(axis, q):
        if axis == "y":
            return {"sp": sp, "tp": q * 2 + core}
        if axis == "x":
            return {"sp": zi * NEAR + q, "tp": tp}
        return {"sp": q * NEAR + xi, "tp": tp}

    own = {"y": yi, "x": xi, "z": zi}

    pairs = [
        (elapsed_h, elapsed_v), (tokens_h, tokens_v), (ngain_h, ngain_v), (rate_h, rate_v), (angle_h, angle_v),
        (sin_h, sin_v), (sout_h, sout_v), (skip_h, skip_v), (gbias_h, gbias_v), (glu_h, glu_v),
        (ogain_h, ogain_v), (outw_h, outw_v),
    ]
    copies = [pltpu.make_async_copy(a, b, dma_sem.at[k]) for k, (a, b) in enumerate(pairs)]
    c_el, c_tok, c_ng, c_rate, c_ang, c_sin, c_sout, c_skip, c_gb, c_glu, c_og, c_ow = copies
    in_copies = [
        pltpu.make_async_copy(inw_h.at[pl.ds(k * 512, 512), :], inw_v.at[pl.ds(k * 512, 512), :], dma_sem.at[12 + k])
        for k in range(4)
    ]
    for c in (c_el, c_tok, c_ng, c_rate, c_ang):
        c.start()
    for c in in_copies:
        c.start()
    for c in (c_sin, c_sout, c_skip, c_gb, c_glu, c_og, c_ow):
        c.start()

    barrier = pltpu.get_barrier_semaphore()
    pl.semaphore_signal(barrier, inc=1, device_id=partner(), device_id_type=MESH)
    for axis in "yxz":
        for k in range(1, NEAR):
            peer = along(axis, lax.rem(own[axis] + k, NEAR))
            pl.semaphore_signal(barrier, inc=1, device_id=peer, device_id_type=MESH)

    c_el.wait()
    steps = elapsed_v[...]
    whole = jnp.floor(steps)
    rest = steps - whole
    lane8 = lax.broadcasted_iota(jnp.int32, (SUBS, 128), 1)
    sub8 = lax.broadcasted_iota(jnp.int32, (SUBS, 128), 0)

    def picked(mask, row):
        total = jnp.sum(jnp.where(mask, jnp.broadcast_to(row, (SUBS, 128)), 0.0), axis=1, keepdims=True)
        return jnp.broadcast_to(total, (SUBS, 128))

    t_own[...] = jnp.where(sub8 == 0, picked(lane8 >= 0, whole), picked(lane8 >= 0, rest))
    for j in range(STEPS):
        dts[j] = picked(lane8 == sub8 * STEPS + j, steps)
    stretch = lane8 // STEPS
    for k, mask in enumerate((stretch == sub8, stretch > sub8, stretch < sub8)):
        spans[2 * k] = picked(mask, whole)
        spans[2 * k + 1] = picked(mask, rest)

    pl.semaphore_wait(barrier, 1 + 3 * (NEAR - 1))

    def t_core():
        return pltpu.make_async_remote_copy(
            src_ref=t_own, dst_ref=t_par, send_sem=t_send.at[0], recv_sem=t_recv.at[0],
            device_id=partner(), device_id_type=MESH,
        )

    def t_stage(axis, buf, base):
        me = own[axis]
        made = []
        for k in range(1, NEAR):
            q = lax.rem(me + k, NEAR)
            made.append(pltpu.make_async_remote_copy(
                src_ref=buf.at[me], dst_ref=buf.at[me], send_sem=t_send.at[base + k],
                recv_sem=t_recv.at[base + me], device_id=along(axis, q), device_id_type=MESH,
            ))
        return made

    def t_arrived(axis, buf, base):
        me = own[axis]
        for k in range(1, NEAR):
            q = lax.rem(me + k, NEAR)
            pltpu.make_async_remote_copy(
                src_ref=buf.at[q], dst_ref=buf.at[q], send_sem=t_send.at[base + k],
                recv_sem=t_recv.at[base + q], device_id=along(axis, q), device_id_type=MESH,
            ).wait_recv()

    t_core().start()

    c_rate.wait()
    c_ang.wait()
    for d in range(2):
        rate = jnp.concatenate([rate_v[d, 0:TILES, :], rate_v[d, TILES:, :]], axis=1)
        angle = jnp.concatenate([angle_v[d, 0:TILES, :], angle_v[d, TILES:, :]], axis=1)
        tabs[d, 0] = rate * (-LOG2E)
        tabs[d, 1] = rate * 2.0
        big = lax.round(angle * 1024.0, lax.RoundingMethod.TO_NEAREST_EVEN) * (1.0 / 1024.0)
        small = angle - big
        first = big * TURN_HI
        second = big * TURN_LO + (small * TURN_HI + small * TURN_LO)
        high = lax.round(first * 256.0, lax.RoundingMethod.TO_NEAREST_EVEN) * (1.0 / 256.0)
        low = (first - high) + second
        tabs[d, 2] = high
        tabs[d, 3] = low
        tabs[d, 4] = high + low

    def stretch_decay(rate2, high, low, both, t_whole, t_rest):
        size = jnp.exp2(rate2 * (t_whole + t_rest))
        turns = high * t_whole
        turns = turns - lax.round(turns, lax.RoundingMethod.TO_NEAREST_EVEN)
        return decay_parts(size, turns + low * t_whole + both * t_rest)

    def table_decay(d, t_tile):
        t_whole = jnp.broadcast_to(t_tile[0:1, :], (TILES, 128))
        t_rest = jnp.broadcast_to(t_tile[1:2, :], (TILES, 128))
        return stretch_decay(tabs[d, 0], tabs[d, 2], tabs[d, 3], tabs[d, 4], t_whole, t_rest)

    c_tok.wait()
    c_ng.wait()
    for r in range(4):
        x = tokens_v[pl.ds(r * 32, 32), :].astype(F32)
        scale = lax.rsqrt(jnp.mean(x * x, axis=-1, keepdims=True) + EPS)
        normed[pl.ds(r * 32, 32), :] = (x * scale * ngain_v[...]).astype(BF16)

    t_core().wait_recv()
    t_y[yi] = t_own[...] + t_par[...]
    for c in t_stage("y", t_y, 1):
        c.start()

    for k in range(2):
        in_copies[k].wait()
        part = jnp.dot(normed[:, k * 512:(k + 1) * 512], inw_v[k * 512:(k + 1) * 512, :], preferred_element_type=F32)
        acc[...] = part if k == 0 else acc[...] + part
    t_arrived("y", t_y, 1)
    t_x[xi] = t_y[0] + t_y[1] + t_y[2] + t_y[3]
    for c in t_stage("x", t_x, 5):
        c.start()
    for k in range(2, 4):
        in_copies[k].wait()
        acc[...] += jnp.dot(normed[:, k * 512:(k + 1) * 512], inw_v[k * 512:(k + 1) * 512, :], preferred_element_type=F32)

    row_i = lax.broadcasted_iota(jnp.int32, (ROWS, ROWS), 0)
    col_i = lax.broadcasted_iota(jnp.int32, (ROWS, ROWS), 1)
    order = jnp.where(col_i == (row_i % SUBS) * STEPS + row_i // SUBS, 1.0, 0.0).astype(BF16)
    back = jnp.where(row_i == (col_i % SUBS) * STEPS + col_i // SUBS, 1.0, 0.0).astype(BF16)

    driven = jnp.dot(order, acc[...].astype(BF16), preferred_element_type=F32)
    c_skip.wait()
    for m in range(4):
        low_d, high_d = driven[:, m * 128:(m + 1) * 128], driven[:, 512 + m * 128:512 + (m + 1) * 128]
        resp[m, :, 0:128] = low_d * skip_v[:, m * 128:(m + 1) * 128]
        resp[m, :, 128:256] = high_d * skip_v[:, 512 + m * 128:512 + (m + 1) * 128]
        drv[m, :, 0:128] = low_d.astype(BF16)
        drv[m, :, 128:256] = high_d.astype(BF16)

    t_arrived("x", t_x, 5)
    t_z[zi] = t_x[0] + t_x[1] + t_x[2] + t_x[3]
    for c in t_stage("z", t_z, 9):
        c.start()

    c_sin.wait()
    nothing = jnp.zeros((128, 64), BF16)
    for m in range(4):
        for d in range(2):
            for part in range(2):
                at = (d * 2 + part) * 128
                lower = sin_v[d, part, m * 8:(m + 1) * 8].reshape(128, 64)
                upper = sin_v[d, part, TILES + m * 8:TILES + (m + 1) * 8].reshape(128, 64)
                bst[m, 0:128, at:at + 128] = jnp.concatenate([lower, nothing], axis=1)
                bst[m, 128:256, at:at + 128] = jnp.concatenate([nothing, upper], axis=1)

    group_lane = (lax.broadcasted_iota(jnp.int32, (ROWS, 256), 1) // 16) % 8

    def project(tile, carry):
        m, i = tile // 8, tile % 8
        lhs = jnp.where(group_lane == i, drv[m].astype(F32), 0.0).astype(BF16)
        proj[tile] = jnp.dot(lhs, bst[m], preferred_element_type=F32)
        return carry

    lax.fori_loop(0, TILES, project, 0)

    def first_pass(tile, carry):
        rows = []
        for d in range(2):
            line = [jnp.broadcast_to(tabs[d, k, pl.ds(tile, 1), :], (SUBS, 128)) for k in range(5)]
            rate2, double, high, low, both = line
            s_re = s_im = None
            base = d * 256
            for j in range(STEPS) if d == 0 else range(STEPS - 1, -1, -1):
                dt = dts[j]
                at = pl.ds(j * SUBS, SUBS)
                size = jnp.exp2(rate2 * dt)
                a_re, a_im = decay_parts(size, both * dt)
                y = double * dt
                near = y * horner(y, (1.0, -0.5, 1.0 / 6.0, -1.0 / 24.0))
                gap = jnp.where(y < 0.03, near, 1.0 - size * size)
                damp = gap * lax.rsqrt(jnp.maximum(gap, 1e-37))
                p_re = proj[tile, at, base:base + 128] * damp
                p_im = proj[tile, at, base + 128:base + 256] * damp
                proj[tile, at, base:base + 128] = p_re
                proj[tile, at, base + 128:base + 256] = p_im
                dec[tile, at, base:base + 128] = a_re
                dec[tile, at, base + 128:base + 256] = a_im
                if s_re is None:
                    s_re, s_im = p_re, p_im
                else:
                    n_re, n_im = times(a_re, a_im, s_re, s_im)
                    s_re, s_im = n_re + p_re, n_im + p_im
            loc[tile, d, 0] = s_re
            loc[tile, d, 1] = s_im
            k = 2 if d == 0 else 4
            w_re, w_im = stretch_decay(rate2, high, low, both, spans[k], spans[k + 1])
            m_re, m_im = times(w_re, w_im, s_re, s_im)
            ssum[d, 0, pl.ds(tile, 1), :] = jnp.sum(m_re, axis=0, keepdims=True)
            ssum[d, 1, pl.ds(tile, 1), :] = jnp.sum(m_im, axis=0, keepdims=True)
        return carry

    lax.fori_loop(0, TILES, first_pass, 0)

    def d_core():
        return pltpu.make_async_remote_copy(
            src_ref=ssum.at[core], dst_ref=s_par, send_sem=d_send.at[0], recv_sem=d_recv.at[0],
            device_id=partner(), device_id_type=MESH,
        )

    def d_stage(axis, buf, base):
        me = own[axis]
        return [
            pltpu.make_async_remote_copy(
                src_ref=buf.at[me], dst_ref=buf.at[me], send_sem=d_send.at[base + k], recv_sem=d_recv.at[base + me],
                device_id=along(axis, lax.rem(me + k, NEAR)), device_id_type=MESH,
            )
            for k in range(1, NEAR)
        ]

    def d_arrived(axis, buf, base):
        me = own[axis]
        for k in range(1, NEAR):
            q = lax.rem(me + k, NEAR)
            pltpu.make_async_remote_copy(
                src_ref=buf.at[q], dst_ref=buf.at[q], send_sem=d_send.at[base + k], recv_sem=d_recv.at[base + q],
                device_id=along(axis, q), device_id_type=MESH,
            ).wait_recv()

    def walk(axis, sbuf, tbuf):
        me = own[axis]
        run = (jnp.zeros((TILES, 128), F32), jnp.zeros((TILES, 128), F32))
        run_d = (jnp.ones((TILES, 128), F32), jnp.zeros((TILES, 128), F32))
        before, before_d = run, run_d
        for o in range(NEAR):
            q = jnp.where(way == 0, o, NEAR - 1 - o)
            here = q == me
            before = tuple(jnp.where(here, a, b) for a, b in zip(run, before))
            before_d = tuple(jnp.where(here, a, b) for a, b in zip(run_d, before_d))
            gain = table_decay(way, tbuf[q])
            moved = times(*gain, *run)
            run = (moved[0] + sbuf[q, 0], moved[1] + sbuf[q, 1])
            run_d = times(*gain, *run_d)
        return before, before_d, run

    d_core().start()
    t_arrived("z", t_z, 9)
    mine = table_decay(way, t_own[...])
    d_core().wait_recv()
    moved = times(*mine, s_par[0], s_par[1])
    s_y[yi, 0] = moved[0] + ssum[way, 0]
    s_y[yi, 1] = moved[1] + ssum[way, 1]
    for c in d_stage("y", s_y, 1):
        c.start()

    def lead_in(tile, carry):
        for d in range(2):
            rate2, _, high, low, both = [
                jnp.broadcast_to(tabs[d, k, pl.ds(tile, 1), :], (SUBS, 128)) for k in range(5)
            ]
            g_re, g_im = stretch_decay(rate2, high, low, both, spans[0], spans[1])
            x_re, x_im = loc[tile, d, 0], loc[tile, d, 1]
            for hop in (1, 2, 4):
                turn = hop if d == 0 else SUBS - hop
                inside = sub8 >= hop if d == 0 else sub8 < SUBS - hop
                q_re, q_im, h_re, h_im = [pltpu.roll(v, turn, 0) for v in (x_re, x_im, g_re, g_im)]
                m_re, m_im = times(g_re, g_im, q_re, q_im)
                n_re, n_im = times(g_re, g_im, h_re, h_im)
                x_re, x_im = jnp.where(inside, x_re + m_re, x_re), jnp.where(inside, x_im + m_im, x_im)
                g_re, g_im = jnp.where(inside, n_re, g_re), jnp.where(inside, n_im, g_im)
            turn = 1 if d == 0 else SUBS - 1
            inside = sub8 >= 1 if d == 0 else sub8 < SUBS - 1
            x_re, x_im, g_re, g_im = [
                jnp.where(inside, pltpu.roll(v, turn, 0), blank_value)
                for v, blank_value in ((x_re, 0.0), (x_im, 0.0), (g_re, 1.0), (g_im, 0.0))
            ]
            lead[tile, d, 0] = x_re
            lead[tile, d, 1] = x_im
            fade[tile, d, 0] = g_re
            fade[tile, d, 1] = g_im
        return carry

    lax.fori_loop(0, TILES, lead_in, 0)

    c_sout.wait()
    lane_group = lax.broadcasted_iota(jnp.int32, (64, 128), 1) // 16
    blank = jnp.zeros((64, 128), BF16)

    def spread(m, carry):
        for d in range(2):
            for part in range(2):
                sign = 1.0 if part == 0 else -1.0
                at = (d * 2 + part) * 128
                lower = (sout_v[d, part, pl.ds(m * 8, 8)].reshape(128, 64) * sign).T
                upper = (sout_v[d, part, pl.ds(TILES + m * 8, 8)].reshape(128, 64) * sign).T
                for i in range(8):
                    tile = m * 8 + i
                    cst[tile, at:at + 64, 0:128] = jnp.where(lane_group == i, lower, 0.0).astype(BF16)
                    cst[tile, at:at + 64, 128:256] = blank
                    cst[tile, at + 64:at + 128, 0:128] = blank
                    cst[tile, at + 64:at + 128, 128:256] = jnp.where(lane_group == i, upper, 0.0).astype(BF16)
        return carry

    lax.fori_loop(0, 4, spread, 0)

    d_arrived("y", s_y, 1)
    y_in, y_fade, line_total = walk("y", s_y, t_y)
    s_x[xi, 0] = line_total[0]
    s_x[xi, 1] = line_total[1]
    for c in d_stage("x", s_x, 5):
        c.start()
    d_arrived("x", s_x, 5)
    x_in, x_fade, plane_total = walk("x", s_x, t_x)
    s_z[zi, 0] = plane_total[0]
    s_z[zi, 1] = plane_total[1]
    for c in d_stage("z", s_z, 9):
        c.start()
    both_fade = times(*y_fade, *x_fade)
    moved = times(*y_fade, *x_in)
    held = (moved[0] + y_in[0], moved[1] + y_in[1])
    other = table_decay(way, t_par[...])
    d_arrived("z", s_z, 9)
    z_in, _, _ = walk("z", s_z, t_z)
    moved = times(*both_fade, *z_in)
    chip = (moved[0] + held[0], moved[1] + held[1])
    s_fin[0] = chip[0]
    s_fin[1] = chip[1]
    last = pltpu.make_async_remote_copy(
        src_ref=s_fin, dst_ref=s_in, send_sem=d_send.at[13], recv_sem=d_recv.at[13],
        device_id=partner(), device_id_type=MESH,
    )
    last.start()
    moved = times(*other, *chip)
    ent[way, 0] = moved[0] + s_par[0]
    ent[way, 1] = moved[1] + s_par[1]
    last.wait_recv()
    ent[core, 0] = s_in[0]
    ent[core, 1] = s_in[1]

    def second_pass(tile, carry):
        parts = []
        for d in range(2):
            base = d * 256
            e_re = jnp.broadcast_to(ent[d, 0, pl.ds(tile, 1), :], (SUBS, 128))
            e_im = jnp.broadcast_to(ent[d, 1, pl.ds(tile, 1), :], (SUBS, 128))
            m_re, m_im = times(fade[tile, d, 0], fade[tile, d, 1], e_re, e_im)
            s_re, s_im = m_re + lead[tile, d, 0], m_im + lead[tile, d, 1]
            found = [None] * STEPS
            for j in range(STEPS) if d == 0 else range(STEPS - 1, -1, -1):
                at = pl.ds(j * SUBS, SUBS)
                n_re, n_im = times(dec[tile, at, base:base + 128], dec[tile, at, base + 128:base + 256], s_re, s_im)
                s_re = n_re + proj[tile, at, base:base + 128]
                s_im = n_im + proj[tile, at, base + 128:base + 256]
                found[j] = (s_re, s_im)
            for part in range(2):
                parts.append(jnp.concatenate([f[part] for f in found], axis=0).astype(BF16))
        states = jnp.concatenate(parts, axis=1)
        m = tile // 8
        resp[m] = resp[m] + jnp.dot(states, cst[tile], preferred_element_type=F32)
        return carry

    lax.fori_loop(0, TILES, second_pass, 0)

    c_gb.wait()
    c_glu.wait()
    response = jnp.concatenate(
        [resp[m, :, 0:128] for m in range(4)] + [resp[m, :, 128:256] for m in range(4)], axis=1
    )
    acc[...] = jax.nn.gelu(response, approximate=True)
    active_low = acc[...].astype(BF16)
    gates = []
    for n in range(4):
        at = slice(n * 256, (n + 1) * 256)
        gate = jnp.dot(active_low, glu_v[:, at], preferred_element_type=F32) + gbias_v[:, at]
        gates.append((acc[:, at] * jax.nn.sigmoid(gate)).astype(BF16))
    gated = jnp.dot(back, jnp.concatenate(gates, axis=1), preferred_element_type=F32).astype(BF16)
    c_og.wait()
    c_ow.wait()
    outs, square = [], None
    for n in range(8):
        at = slice(n * 256, (n + 1) * 256)
        piece = jnp.dot(gated, outw_v[:, at], preferred_element_type=F32)
        outs.append(piece)
        part = jnp.sum(piece * piece, axis=-1, keepdims=True)
        square = part if square is None else square + part
    scale = lax.rsqrt(square * (1.0 / 2048.0) + EPS)
    for n in range(8):
        at = slice(n * 256, (n + 1) * 256)
        out_ref[:, at] = (outs[n] * scale * ogain_v[:, at]).astype(BF16)

    t_core().wait_send()
    d_core().wait_send()
    for axis, tb, sb, base in (("y", t_y, s_y, 1), ("x", t_x, s_x, 5), ("z", t_z, s_z, 9)):
        for c in t_stage(axis, tb, base) + d_stage(axis, sb, base):
            c.wait_send()
    last.wait_send()


def local(
    tokens, elapsed, norm_gain, in_weight, state_input, state_output, forget_rate, decay_angle,
    skip_gain, glu_weight, glu_bias, out_weight, out_gain,
):
    args = (
        tokens, elapsed.reshape(1, -1), norm_gain.reshape(1, -1), in_weight, state_input.transpose(0, 1, 2, 4, 3),
        state_output, forget_rate, decay_angle, skip_gain.reshape(1, -1), glu_weight, glu_bias.reshape(1, -1),
        out_weight, out_gain.reshape(1, -1),
    )
    vm = pltpu.VMEM
    scratch = [vm(a.shape, a.dtype) for a in args]
    scratch += [
        vm((ROWS, 2048), BF16),
        vm((ROWS, 1024), F32),
        vm((4, ROWS, 256), BF16),
        vm((4, ROWS, 256), F32),
        vm((4, 256, 512), BF16),
        vm((TILES, 512, 256), BF16),
        vm((TILES, ROWS, 512), F32),
        vm((TILES, ROWS, 512), F32),
        vm((2, 5, TILES, 128), F32),
        vm((STEPS, SUBS, 128), F32),
        vm((6, SUBS, 128), F32),
        vm((TILES, 2, 2, SUBS, 128), F32),
        vm((2, 2, TILES, 128), F32),
        vm((TILES, 2, 2, SUBS, 128), F32),
        vm((TILES, 2, 2, SUBS, 128), F32),
        vm((2, 2, TILES, 128), F32),
        vm((8, 128), F32), vm((8, 128), F32),
        vm((4, 8, 128), F32), vm((4, 8, 128), F32), vm((4, 8, 128), F32),
        vm((2, TILES, 128), F32),
        vm((4, 2, TILES, 128), F32), vm((4, 2, TILES, 128), F32), vm((4, 2, TILES, 128), F32),
        vm((2, TILES, 128), F32), vm((2, TILES, 128), F32),
        pltpu.SemaphoreType.DMA((16,)),
        pltpu.SemaphoreType.DMA((14,)), pltpu.SemaphoreType.DMA((14,)),
        pltpu.SemaphoreType.DMA((14,)), pltpu.SemaphoreType.DMA((14,)),
    ]
    return pl.pallas_call(
        kernel,
        out_shape=jax.ShapeDtypeStruct(tokens.shape, BF16),
        in_specs=[pl.BlockSpec(memory_space=pl.ANY)] * len(args),
        out_specs=pl.BlockSpec(memory_space=pltpu.VMEM),
        scratch_shapes=scratch,
        compiler_params=pltpu.CompilerParams(
            collective_id=0, has_side_effects=True, vmem_limit_bytes=67000000
        ),
        name="ssm_layer",
    )(*args)


def solution(mesh):
    rows = P(("sp", "tp"), None)
    placed = (rows, P(("sp", "tp")), P(), P(), P(), P(), P(), P(), P(), P(), P(), P(), P())
    return jax.shard_map(local, mesh=mesh, in_specs=placed, out_specs=rows, check_vma=False)
```

profile of v0, /device:TPU:1, one launch (start us, length us, event | category | flops | bytes accessed | tf_op | source)
XLA Modules:
  0.0 55.3 jit_solution(4205904472193167573)
XLA Ops:
  0.0 53.4 %ssm_layer.1 = bf16[128,2048]{1,0:T(8,128)(2,1)} custom-call(bf16[128,2048]{1,0:T(8,128)(2,1)} %tokens_h.1, f32[1,128]{1,0:T(1,128)} %bitcast.11, f32[1,2048]{1,0:T(1,128)} %bitcast.7, bf16[2048,1024]{1,0:T(8,128)(2,1)} %inw_h.1, bf16[2,2,64,16,64]{4,3,2,1,0:T(8,128)(2,1)} %bitcast.6, f32[2,2,64,16,64]{4,3,2,1,0:T(8,128)} %sout_h.1, f32[2,64,64]{2,1,0:T(8,128)} %rate_h.1, ...), custom_call_target="tpu_custom_call" | custom-call | tf_op jit(solution)/shard_map/ssm_layer/pallas_call | solution.py:513
  53.4 1.9 %copy.15 = bf16[128,2048]{1,0:T(8,128)(2,1)} copy(bf16[128,2048]{1,0:T(8,128)(2,1)} %ssm_layer.1) | data formatting | bytes 1048576
where the time goes:
time: 55.4 us; the launch traced here: 55.3 us
  Pallas kernels  53.4 us (96%)
  local copies, waits for them, and re-layouts  1.88 us (3%)
    pallas_call x1, Pallas kernels, local(): pl.pallas_call(kernel, out_shape=jax.ShapeDtypeStruct(tokens.shape, BF16)...  53.4 us
    unnamed x1, local copies, waits for them, and re-layouts  1.88 us

commit v1 on v0

v1 whole, which is shorter than its diff:
```python
import functools
import math

import jax
import jax.numpy as jnp
from jax import lax
from jax.experimental import pallas as pl
from jax.experimental.pallas import tpu as pltpu
from jax.sharding import PartitionSpec as P

F32 = jnp.float32
BF16 = jnp.bfloat16
MESH = pl.DeviceIdType.MESH

ROWS = 128
TILES = 32
SUBS = 8
STEPS = 16
LINE = 8
LINES = 16
QUARTER = 8
EPS = 1e-06
LOG2E = 1.4426950408889634
SIN_C = (4.442883014678955, -7.308241367340088, 3.6062889099121094, -0.845763623714447, 0.10920575261116028)
COS_C = (1.4142135381698608, -6.9788641929626465, 5.73988151550293, -1.8882750272750854, 0.3322518765926361, -0.034502167254686356)
POINTS = [1.5 + 1.5 * math.cos((2 * i + 1) * math.pi / 32.0) for i in range(16)]
WEIGHTS = [1.0 / math.prod(p - o for o in POINTS if o != p) for p in POINTS]
INV_TURN = 1.0 / (2.0 * math.pi)
TURN_HI = math.floor(INV_TURN * 4096.0) / 4096.0
TURN_LO = INV_TURN - TURN_HI


def horner(x, coefficients):
    total = coefficients[-1]
    for c in coefficients[-2::-1]:
        total = total * x + c
    return total


def half_turn_parts(turns):
    part = turns - lax.round(turns, lax.RoundingMethod.TO_NEAREST_EVEN)
    square = part * part
    return part * horner(square, SIN_C), horner(square, COS_C)


def decay_parts(size, turns):
    sine, cosine = half_turn_parts(turns)
    lean = size * sine
    return size - lean * sine, lean * cosine


def in_parts(value, count):
    parts = []
    for _ in range(count):
        parts.append(value.astype(BF16))
        value = value - parts[-1].astype(F32)
    return parts


def times(a_re, a_im, b_re, b_im):
    return a_re * b_re - a_im * b_im, a_re * b_im + a_im * b_re


def kernel(
    tokens_h, elapsed_h, ngain_h, inw_h, sin_h, sout_h, rate_h, angle_h, skip_h, glu_h, gbias_h, outw_h, ogain_h,
    out_ref,
    tokens_v, elapsed_v, ngain_v, inw_v, sin_v, sout_v, rate_v, angle_v, skip_v, glu_v, gbias_v, outw_v, ogain_v,
    normed, acc, drv, resp, bst, cst, proj, dec, tabs, by_token, at_node, cell_decay, cell_gain, gain, states, spans, loc, ssum, lead, fade,
    t_dev, t_line, g_in, x_in, x_far, e_new, e_fade, e_in,
    dma_sem, t_send, t_recv, u_send, u_recv, g_send, g_recv, x_send, x_recv, e_send, e_recv,
):
    sp = lax.axis_index("sp")
    tp = lax.axis_index("tp")
    yi, core = tp // 2, tp % 2
    way = 1 - core

    def line_peer(k):
        return {"sp": sp, "tp": k}

    def plane_peer(k):
        return {"sp": k, "tp": tp}

    def remote(src, dst, send_sem, recv_sem, peer):
        return pltpu.make_async_remote_copy(
            src_ref=src, dst_ref=dst, send_sem=send_sem, recv_sem=recv_sem, device_id=peer, device_id_type=MESH,
        )

    def ahead(step):
        k = jnp.where(way == 0, sp + step, sp - step)
        return lax.rem(k + LINES, LINES), jnp.logical_and(k >= 0, k < LINES)

    def behind(step):
        return ahead(-step)

    pairs = [
        (elapsed_h, elapsed_v), (tokens_h, tokens_v), (ngain_h, ngain_v), (rate_h, rate_v), (angle_h, angle_v),
        (sin_h, sin_v), (sout_h, sout_v), (skip_h, skip_v), (gbias_h, gbias_v), (glu_h, glu_v),
        (ogain_h, ogain_v), (outw_h, outw_v),
    ]
    copies = [pltpu.make_async_copy(a, b, dma_sem.at[k]) for k, (a, b) in enumerate(pairs)]
    c_el, c_tok, c_ng, c_rate, c_ang, c_sin, c_sout, c_skip, c_gb, c_glu, c_og, c_ow = copies
    in_copies = [
        pltpu.make_async_copy(inw_h.at[pl.ds(k * 512, 512), :], inw_v.at[pl.ds(k * 512, 512), :], dma_sem.at[12 + k])
        for k in range(4)
    ]
    for c in (c_el, c_tok, c_ng, c_rate, c_ang):
        c.start()
    for c in in_copies:
        c.start()
    for c in (c_sin, c_sout, c_skip, c_gb, c_glu, c_og, c_ow):
        c.start()

    barrier = pltpu.get_barrier_semaphore()
    for k in range(1, LINE):
        pl.semaphore_signal(barrier, inc=1, device_id=line_peer(lax.rem(tp + k, LINE)), device_id_type=MESH)
    for k in range(1, LINES):
        pl.semaphore_signal(barrier, inc=1, device_id=plane_peer(lax.rem(sp + k, LINES)), device_id_type=MESH)

    c_el.wait()
    steps = elapsed_v[...]
    whole = jnp.floor(steps)
    rest = steps - whole
    lane8 = lax.broadcasted_iota(jnp.int32, (SUBS, 128), 1)
    sub8 = lax.broadcasted_iota(jnp.int32, (SUBS, 128), 0)

    def picked(mask, row):
        total = jnp.sum(jnp.where(mask, jnp.broadcast_to(row, (SUBS, 128)), 0.0), axis=1, keepdims=True)
        return jnp.broadcast_to(total, (SUBS, 128))

    t_dev[tp] = jnp.where(sub8 == 0, picked(lane8 >= 0, whole), picked(lane8 >= 0, rest))
    gaps = [steps - p for p in POINTS]
    upto, after = [jnp.ones_like(steps)], [jnp.ones_like(steps)]
    for k in range(15):
        upto.append(upto[-1] * gaps[k])
        after.append(after[-1] * gaps[15 - k])
    basis = [upto[k] * after[15 - k] * WEIGHTS[k] for k in range(16)]
    scale = basis[0]
    for b in basis[1:]:
        scale = scale + b
    basis = jnp.concatenate(basis, axis=0) / jnp.broadcast_to(scale, (16, 128))
    b1, b2, b3 = in_parts(basis, 3)
    r1, r2 = in_parts(basis * jnp.sqrt(steps), 2)
    none16 = jnp.zeros((16, 128), BF16)
    token_rows = jnp.concatenate([b1, b1, b2, b2, b1, b3, none16, none16], axis=0)
    gain_rows = jnp.concatenate([r1, r1, r2] + [none16] * 5, axis=0)
    row_i = lax.broadcasted_iota(jnp.int32, (ROWS, ROWS), 0)
    col_i = lax.broadcasted_iota(jnp.int32, (ROWS, ROWS), 1)
    order = jnp.where(col_i == (row_i % SUBS) * STEPS + row_i // SUBS, 1.0, 0.0).astype(BF16)
    back = jnp.where(row_i == (col_i % SUBS) * STEPS + col_i // SUBS, 1.0, 0.0).astype(BF16)
    across = (((1,), (1,)), ((), ()))
    for k, rows in enumerate((token_rows, gain_rows)):
        by_token[k] = lax.dot_general(order, rows, across, preferred_element_type=F32).astype(BF16)
    node_i = lax.broadcasted_iota(jnp.int32, (16, 128), 0)
    nodes = jnp.full((16, 128), POINTS[0], F32)
    for k in range(1, 16):
        nodes = jnp.where(node_i == k, POINTS[k], nodes)
    at_node[...] = nodes
    none32 = jnp.zeros((32, 512), BF16)
    none80 = jnp.zeros((80, 256), BF16)
    for t in range(QUARTER):
        cell_decay[t, 96:128, :] = none32
        cell_gain[t, 48:128, :] = none80
    stretch = lane8 // STEPS
    for k, mask in enumerate((stretch == sub8, stretch > sub8, stretch < sub8)):
        spans[2 * k] = picked(mask, whole)
        spans[2 * k + 1] = picked(mask, rest)

    def t_out(k):
        peer = lax.rem(tp + k, LINE)
        return remote(t_dev.at[tp], t_dev.at[tp], t_send.at[k], t_recv.at[tp], line_peer(peer))

    def t_in(k):
        peer = lax.rem(tp + k, LINE)
        return remote(t_dev.at[peer], t_dev.at[peer], t_send.at[k], t_recv.at[peer], line_peer(peer))

    def u_out(k, peer):
        return remote(t_line.at[sp], t_line.at[sp], u_send.at[k], u_recv.at[sp], plane_peer(peer))

    def u_in(k, peer):
        return remote(t_line.at[peer], t_line.at[peer], u_send.at[k], u_recv.at[peer], plane_peer(peer))

    def x_out(k, peer):
        return remote(x_in.at[sp], x_in.at[sp], x_send.at[k], x_recv.at[sp], plane_peer(peer))

    def x_arr(k, peer):
        return remote(x_in.at[peer], x_in.at[peer], x_send.at[k], x_recv.at[peer], plane_peer(peer))

    def g_out(d, q):
        return remote(ssum.at[d, q], g_in.at[tp], g_send.at[q * 2 + d], g_recv.at[tp], line_peer(q * 2 + 1 - d))

    def g_arr(k):
        peer = lax.rem(tp + k, LINE)
        return remote(ssum.at[0, 0], g_in.at[peer], g_send.at[k], g_recv.at[peer], line_peer(peer))

    def e_out(k):
        peer = lax.rem(tp + k, LINE)
        return remote(e_new.at[peer], e_in.at[tp], e_send.at[k], e_recv.at[tp], line_peer(peer))

    def e_arr(k):
        peer = lax.rem(tp + k, LINE)
        return remote(e_new.at[peer], e_in.at[peer], e_send.at[k], e_recv.at[peer], line_peer(peer))

    c_rate.wait()
    c_ang.wait()
    for d in range(2):
        rate = jnp.concatenate([rate_v[d, 0:TILES, :], rate_v[d, TILES:, :]], axis=1)
        angle = jnp.concatenate([angle_v[d, 0:TILES, :], angle_v[d, TILES:, :]], axis=1)
        tabs[d, 0] = rate * (-LOG2E)
        tabs[d, 1] = rate * 2.0
        big = lax.round(angle * 1024.0, lax.RoundingMethod.TO_NEAREST_EVEN) * (1.0 / 1024.0)
        small = angle - big
        first = big * TURN_HI
        second = big * TURN_LO + (small * TURN_HI + small * TURN_LO)
        high = lax.round(first * 256.0, lax.RoundingMethod.TO_NEAREST_EVEN) * (1.0 / 256.0)
        low = (first - high) + second
        tabs[d, 2] = high
        tabs[d, 3] = low
        tabs[d, 4] = high + low

    def stretch_decay(rate2, high, low, both, t_whole, t_rest):
        size = jnp.exp2(rate2 * (t_whole + t_rest))
        turns = high * t_whole
        turns = turns - lax.round(turns, lax.RoundingMethod.TO_NEAREST_EVEN)
        return decay_parts(size, turns + low * t_whole + both * t_rest)

    def quarter_decay(t_tile):
        t_whole = jnp.broadcast_to(t_tile[0:1, :], (QUARTER, 128))
        t_rest = jnp.broadcast_to(t_tile[1:2, :], (QUARTER, 128))
        rows = pl.ds(pl.multiple_of(yi * QUARTER, QUARTER), QUARTER)
        return stretch_decay(*[tabs[way, k, rows, :] for k in (0, 2, 3, 4)], t_whole, t_rest)

    c_tok.wait()
    c_ng.wait()
    for r in range(4):
        x = tokens_v[pl.ds(r * 32, 32), :].astype(F32)
        scale = lax.rsqrt(jnp.mean(x * x, axis=-1, keepdims=True) + EPS)
        normed[pl.ds(r * 32, 32), :] = (x * scale * ngain_v[...]).astype(BF16)

    for k in range(4):
        in_copies[k].wait()
        part = jnp.dot(normed[:, k * 512:(k + 1) * 512], inw_v[k * 512:(k + 1) * 512, :], preferred_element_type=F32)
        acc[...] = part if k == 0 else acc[...] + part

    driven = jnp.dot(order, acc[...].astype(BF16), preferred_element_type=F32)
    c_skip.wait()
    for m in range(4):
        low_d, high_d = driven[:, m * 128:(m + 1) * 128], driven[:, 512 + m * 128:512 + (m + 1) * 128]
        resp[m, :, 0:128] = low_d * skip_v[:, m * 128:(m + 1) * 128]
        resp[m, :, 128:256] = high_d * skip_v[:, 512 + m * 128:512 + (m + 1) * 128]
        drv[m, :, 0:128] = low_d.astype(BF16)
        drv[m, :, 128:256] = high_d.astype(BF16)

    pl.semaphore_wait(barrier, LINE - 1 + LINES - 1)
    for k in range(1, LINE):
        t_out(k).start()

    c_sin.wait()
    nothing = jnp.zeros((128, 64), BF16)
    for m in range(4):
        for d in range(2):
            for part in range(2):
                at = (d * 2 + part) * 128
                lower = sin_v[d, part, m * 8:(m + 1) * 8].reshape(128, 64)
                upper = sin_v[d, part, TILES + m * 8:TILES + (m + 1) * 8].reshape(128, 64)
                bst[m, 0:128, at:at + 128] = jnp.concatenate([lower, nothing], axis=1)
                bst[m, 128:256, at:at + 128] = jnp.concatenate([nothing, upper], axis=1)

    group_lane = (lax.broadcasted_iota(jnp.int32, (ROWS, 256), 1) // 16) % 8

    def first_pass(q, carry):
        def values_at_nodes(t):
            row = pl.ds(q * QUARTER + t, 1)
            x = at_node[...]
            for d in range(2):
                rate2, double, both = [jnp.broadcast_to(tabs[d, k, row, :], (16, 128)) for k in (0, 1, 4)]
                size = jnp.exp2(rate2 * x)
                y = double * x
                near = y * horner(y, (1.0, -0.5, 1.0 / 6.0, -1.0 / 24.0))
                gap = jnp.where(y < 0.03, near, 1.0 - size * size)
                for part, value in enumerate(decay_parts(size, both * x)):
                    v1, v2, v3 = in_parts(value, 3)
                    at = slice((d * 2 + part) * 128, (d * 2 + part + 1) * 128)
                    for k, v in enumerate((v1, v2, v1, v2, v3, v1)):
                        cell_decay[t, k * 16:(k + 1) * 16, at] = v
                g1, g2 = in_parts(gap * lax.rsqrt(jnp.maximum(gap * x, 1e-37)), 2)
                for k, v in enumerate((g1, g2, g1)):
                    cell_gain[t, k * 16:(k + 1) * 16, d * 128:(d + 1) * 128] = v

        def products(t):
            tile = q * QUARTER + t
            dec[tile] = jnp.dot(by_token[0], cell_decay[t], preferred_element_type=F32)
            gain[t] = jnp.dot(by_token[1], cell_gain[t], preferred_element_type=F32)
            lhs = drv[q] * jnp.where(group_lane == t, 1.0, 0.0).astype(BF16)
            proj[tile] = jnp.dot(lhs, bst[q], preferred_element_type=F32)

        def scan(t):
            tile = q * QUARTER + t
            for d in range(2):
                s_re = s_im = None
                base = d * 256
                for j in range(STEPS) if d == 0 else range(STEPS - 1, -1, -1):
                    at = pl.ds(j * SUBS, SUBS)
                    damp = gain[t, at, d * 128:(d + 1) * 128]
                    p_re = proj[tile, at, base:base + 128] * damp
                    p_im = proj[tile, at, base + 128:base + 256] * damp
                    proj[tile, at, base:base + 128] = p_re
                    proj[tile, at, base + 128:base + 256] = p_im
                    if s_re is None:
                        s_re, s_im = p_re, p_im
                    else:
                        a_re, a_im = dec[tile, at, base:base + 128], dec[tile, at, base + 128:base + 256]
                        n_re, n_im = times(a_re, a_im, s_re, s_im)
                        s_re, s_im = n_re + p_re, n_im + p_im
                loc[tile, d, 0] = s_re
                loc[tile, d, 1] = s_im
                k = 2 if d == 0 else 4
                rate2, high, low, both = [
                    jnp.broadcast_to(tabs[d, i, pl.ds(tile, 1), :], (SUBS, 128)) for i in (0, 2, 3, 4)
                ]
                w_re, w_im = stretch_decay(rate2, high, low, both, spans[k], spans[k + 1])
                m_re, m_im = times(w_re, w_im, s_re, s_im)
                ssum[d, q, 0, t:t + 1, :] = jnp.sum(m_re, axis=0, keepdims=True)
                ssum[d, q, 1, t:t + 1, :] = jnp.sum(m_im, axis=0, keepdims=True)

        @pl.when(q == 2)
        def _():
            for k in range(1, LINE):
                t_in(k).wait_recv()
            total = t_dev[0]
            for k in range(1, LINE):
                total = total + t_dev[k]
            t_line[sp] = total
            for k in range(1, LINES):
                peer, there = ahead(k)
                pl.when(there)(u_out(k, peer).start)

        values_at_nodes(0)
        products(0)
        values_at_nodes(1)
        for t in range(QUARTER):
            if t + 1 < QUARTER:
                products(t + 1)
            if t + 2 < QUARTER:
                values_at_nodes(t + 2)
            scan(t)
        for d in range(2):
            pl.when(tp != q * 2 + 1 - d)(g_out(d, q).start)
        return carry

    lax.fori_loop(0, TILES // QUARTER, first_pass, 0)

    def lead_in(tile, carry):
        for d in range(2):
            rate2, _, high, low, both = [
                jnp.broadcast_to(tabs[d, k, pl.ds(tile, 1), :], (SUBS, 128)) for k in range(5)
            ]
            g_re, g_im = stretch_decay(rate2, high, low, both, spans[0], spans[1])
            x_re, x_im = loc[tile, d, 0], loc[tile, d, 1]
            for hop in (1, 2, 4):
                turn = hop if d == 0 else SUBS - hop
                inside = sub8 >= hop if d == 0 else sub8 < SUBS - hop
                q_re, q_im, h_re, h_im = [pltpu.roll(v, turn, 0) for v in (x_re, x_im, g_re, g_im)]
                m_re, m_im = times(g_re, g_im, q_re, q_im)
                n_re, n_im = times(g_re, g_im, h_re, h_im)
                x_re, x_im = jnp.where(inside, x_re + m_re, x_re), jnp.where(inside, x_im + m_im, x_im)
                g_re, g_im = jnp.where(inside, n_re, g_re), jnp.where(inside, n_im, g_im)
            turn = 1 if d == 0 else SUBS - 1
            inside = sub8 >= 1 if d == 0 else sub8 < SUBS - 1
            x_re, x_im, g_re, g_im = [
                jnp.where(inside, pltpu.roll(v, turn, 0), blank_value)
                for v, blank_value in ((x_re, 0.0), (x_im, 0.0), (g_re, 1.0), (g_im, 0.0))
            ]
            lead[tile, d, 0] = x_re
            lead[tile, d, 1] = x_im
            fade[tile, d, 0] = g_re
            fade[tile, d, 1] = g_im
        return carry

    lax.fori_loop(0, TILES, lead_in, 0)

    c_sout.wait()
    lane_group = lax.broadcasted_iota(jnp.int32, (64, 128), 1) // 16
    blank = jnp.zeros((64, 128), BF16)

    def spread(m, carry):
        for d in range(2):
            for part in range(2):
                sign = 1.0 if part == 0 else -1.0
                at = (d * 2 + part) * 128
                lower = (sout_v[d, part, pl.ds(m * 8, 8)].reshape(128, 64) * sign).T
                upper = (sout_v[d, part, pl.ds(TILES + m * 8, 8)].reshape(128, 64) * sign).T
                for i in range(8):
                    tile = m * 8 + i
                    cst[tile, at:at + 64, 0:128] = jnp.where(lane_group == i, lower, 0.0).astype(BF16)
                    cst[tile, at:at + 64, 128:256] = blank
                    cst[tile, at + 64:at + 128, 0:128] = blank
                    cst[tile, at + 64:at + 128, 128:256] = jnp.where(lane_group == i, upper, 0.0).astype(BF16)
        return carry

    lax.fori_loop(0, 4, spread, 0)

    g_in[tp] = ssum[way, yi]
    for k in range(1, LINES):
        peer, there = behind(k)
        pl.when(there)(u_in(k, peer).wait_recv)
    places = [jnp.where(way == 0, o, LINE - 1 - o) for o in range(LINE)]
    gains = [quarter_decay(t_dev[k]) for k in places]
    for k in range(1, LINE):
        g_arr(k).wait_recv()
    zero, one = jnp.zeros((QUARTER, 128), F32), jnp.ones((QUARTER, 128), F32)
    run, run_d, before, before_d = (zero, zero), (one, zero), [], []
    for o, k in enumerate(places):
        before.append(run)
        before_d.append(run_d)
        moved = times(*gains[o], *run)
        run = (moved[0] + g_in[k, 0], moved[1] + g_in[k, 1])
        run_d = times(*gains[o], *run_d)
    x_in[sp, 0] = run[0]
    x_in[sp, 1] = run[1]
    for k in range(1, LINES):
        peer, there = ahead(k)
        pl.when(there)(x_out(k, peer).start)
    for o, k in enumerate(places):
        e_new[k, 0] = before[o][0]
        e_new[k, 1] = before[o][1]
        e_fade[k, 0] = before_d[o][0]
        e_fade[k, 1] = before_d[o][1]
    between = jnp.zeros((SUBS, 128), F32)
    for k in range(1, LINES):
        peer, there = behind(k)
        far_re, far_im = quarter_decay(between)
        x_far[k, 0] = far_re
        x_far[k, 1] = far_im
        between = between + jnp.where(there, t_line[peer], 0.0)

    def local_pass(q, carry):
        total = resp[q]
        for t in range(QUARTER):
            tile = q * QUARTER + t
            for d in range(2):
                base = d * 256
                s_re, s_im = lead[tile, d, 0], lead[tile, d, 1]
                f_re, f_im = fade[tile, d, 0], fade[tile, d, 1]
                found = [None] * STEPS
                for j in range(STEPS) if d == 0 else range(STEPS - 1, -1, -1):
                    at = pl.ds(j * SUBS, SUBS)
                    a_re, a_im = dec[tile, at, base:base + 128], dec[tile, at, base + 128:base + 256]
                    n_re, n_im = times(a_re, a_im, s_re, s_im)
                    s_re = n_re + proj[tile, at, base:base + 128]
                    s_im = n_im + proj[tile, at, base + 128:base + 256]
                    f_re, f_im = times(a_re, a_im, f_re, f_im)
                    dec[tile, at, base:base + 128] = f_re
                    dec[tile, at, base + 128:base + 256] = f_im
                    found[j] = (s_re, s_im)
                    if j % 2 == (1 if d == 0 else 0):
                        first = j - j % 2
                        for part in range(2):
                            pair = jnp.concatenate([found[first][part], found[first + 1][part]], axis=0)
                            states[t, first * SUBS:(first + 2) * SUBS, base + part * 128:base + part * 128 + 128] = (
                                pair.astype(BF16)
                            )
            if t:
                total = total + jnp.dot(states[t - 1], cst[tile - 1], preferred_element_type=F32)
        resp[q] = total + jnp.dot(states[QUARTER - 1], cst[q * QUARTER + QUARTER - 1], preferred_element_type=F32)
        return carry

    lax.fori_loop(0, TILES // QUARTER, local_pass, 0)

    gone = (zero, zero)
    for k in range(1, LINES):
        peer, there = behind(k)
        pl.when(there)(x_arr(k, peer).wait_recv)
        moved = times(x_far[k, 0], x_far[k, 1], x_in[peer, 0], x_in[peer, 1])
        gone = tuple(g + jnp.where(there, m, 0.0) for g, m in zip(gone, moved))
    for k in range(LINE):
        moved = times(e_fade[k, 0], e_fade[k, 1], *gone)
        e_new[k, 0] = e_new[k, 0] + moved[0]
        e_new[k, 1] = e_new[k, 1] + moved[1]
    for k in range(1, LINE):
        e_out(k).start()
    e_in[tp] = e_new[tp]
    for k in range(1, LINE):
        e_arr(k).wait_recv()

    def second_pass(q, carry):
        total = resp[q]
        for t in range(QUARTER):
            tile = q * QUARTER + t
            for d in range(2):
                base = d * 256
                e_re = jnp.broadcast_to(e_in[q * 2 + 1 - d, 0, t:t + 1, :], (16, 128))
                e_im = jnp.broadcast_to(e_in[q * 2 + 1 - d, 1, t:t + 1, :], (16, 128))
                for r in range(0, ROWS, 16):
                    f_re, f_im = dec[tile, r:r + 16, base:base + 128], dec[tile, r:r + 16, base + 128:base + 256]
                    m_re, m_im = times(f_re, f_im, e_re, e_im)
                    states[t, r:r + 16, base:base + 128] = m_re.astype(BF16)
                    states[t, r:r + 16, base + 128:base + 256] = m_im.astype(BF16)
            if t:
                total = total + jnp.dot(states[t - 1], cst[tile - 1], preferred_element_type=F32)
        resp[q] = total + jnp.dot(states[QUARTER - 1], cst[q * QUARTER + QUARTER - 1], preferred_element_type=F32)
        return carry

    lax.fori_loop(0, TILES // QUARTER, second_pass, 0)

    c_gb.wait()
    c_glu.wait()
    response = jnp.concatenate(
        [resp[m, :, 0:128] for m in range(4)] + [resp[m, :, 128:256] for m in range(4)], axis=1
    )
    acc[...] = jax.nn.gelu(response, approximate=True)
    active_low = acc[...].astype(BF16)
    gates = []
    for n in range(4):
        at = slice(n * 256, (n + 1) * 256)
        gate = jnp.dot(active_low, glu_v[:, at], preferred_element_type=F32) + gbias_v[:, at]
        gates.append((acc[:, at] * jax.nn.sigmoid(gate)).astype(BF16))
    gated = jnp.dot(back, jnp.concatenate(gates, axis=1), preferred_element_type=F32).astype(BF16)
    c_og.wait()
    c_ow.wait()
    outs, square = [], None
    for n in range(8):
        at = slice(n * 256, (n + 1) * 256)
        piece = jnp.dot(gated, outw_v[:, at], preferred_element_type=F32)
        outs.append(piece)
        part = jnp.sum(piece * piece, axis=-1, keepdims=True)
        square = part if square is None else square + part
    scale = lax.rsqrt(square * (1.0 / 2048.0) + EPS)
    for n in range(8):
        at = slice(n * 256, (n + 1) * 256)
        out_ref[:, at] = (outs[n] * scale * ogain_v[:, at]).astype(BF16)

    for k in range(1, LINE):
        t_out(k).wait_send()
        e_out(k).wait_send()
    for q in range(TILES // QUARTER):
        for d in range(2):
            pl.when(tp != q * 2 + 1 - d)(g_out(d, q).wait_send)
    for k in range(1, LINES):
        peer, there = ahead(k)
        pl.when(there)(u_out(k, peer).wait_send)
        pl.when(there)(x_out(k, peer).wait_send)


def local(
    tokens, elapsed, norm_gain, in_weight, state_input, state_output, forget_rate, decay_angle,
    skip_gain, glu_weight, glu_bias, out_weight, out_gain,
):
    args = (
        tokens, elapsed.reshape(1, -1), norm_gain.reshape(1, -1), in_weight, state_input.transpose(0, 1, 2, 4, 3),
        state_output, forget_rate, decay_angle, skip_gain.reshape(1, -1), glu_weight, glu_bias.reshape(1, -1),
        out_weight, out_gain.reshape(1, -1),
    )
    vm = pltpu.VMEM
    scratch = [vm(a.shape, a.dtype) for a in args]
    scratch += [
        vm((ROWS, 2048), BF16),
        vm((ROWS, 1024), F32),
        vm((4, ROWS, 256), BF16),
        vm((4, ROWS, 256), F32),
        vm((4, 256, 512), BF16),
        vm((TILES, 512, 256), BF16),
        vm((TILES, ROWS, 512), F32),
        vm((TILES, ROWS, 512), F32),
        vm((2, 5, TILES, 128), F32),
        vm((2, ROWS, 128), BF16),
        vm((16, 128), F32),
        vm((QUARTER, 128, 512), BF16),
        vm((QUARTER, 128, 256), BF16),
        vm((QUARTER, ROWS, 256), F32),
        vm((QUARTER, ROWS, 512), BF16),
        vm((6, SUBS, 128), F32),
        vm((TILES, 2, 2, SUBS, 128), F32),
        vm((2, 4, 2, QUARTER, 128), F32),
        vm((TILES, 2, 2, SUBS, 128), F32),
        vm((TILES, 2, 2, SUBS, 128), F32),
        vm((LINE, SUBS, 128), F32),
        vm((LINES, SUBS, 128), F32),
        vm((LINE, 2, QUARTER, 128), F32),
        vm((LINES, 2, QUARTER, 128), F32),
        vm((LINES, 2, QUARTER, 128), F32),
        vm((LINE, 2, QUARTER, 128), F32),
        vm((LINE, 2, QUARTER, 128), F32),
        vm((LINE, 2, QUARTER, 128), F32),
        pltpu.SemaphoreType.DMA((16,)),
    ]
    for count in (LINE, LINES, LINE, LINES, LINE):
        scratch += [pltpu.SemaphoreType.DMA((count,)), pltpu.SemaphoreType.DMA((count,))]
    return pl.pallas_call(
        kernel,
        out_shape=jax.ShapeDtypeStruct(tokens.shape, BF16),
        in_specs=[pl.BlockSpec(memory_space=pl.ANY)] * len(args),
        out_specs=pl.BlockSpec(memory_space=pltpu.VMEM),
        scratch_shapes=scratch,
        compiler_params=pltpu.CompilerParams(
            collective_id=0, has_side_effects=True, vmem_limit_bytes=67000000
        ),
        name="ssm_layer",
    )(*args)


def solution(mesh):
    rows = P(("sp", "tp"), None)
    placed = (rows, P(("sp", "tp")), P(), P(), P(), P(), P(), P(), P(), P(), P(), P(), P())
    return jax.shard_map(local, mesh=mesh, in_specs=placed, out_specs=rows, check_vma=False)
```

time: 55.4 us -> 34.3 us (0.62)
  Pallas kernels: 53.4 us -> 32.3 us
    pallas_call x1, Pallas kernels: 53.4 us -> 32.3 us  [local(): pl.pallas_call(kernel, out_shape=jax.ShapeDtypeStruct(tokens.shape, BF16)...]
where the time goes in v1:
time: 34.3 us; the launch traced here: 34.1 us
  Pallas kernels  32.3 us (94%)
  local copies, waits for them, and re-layouts  1.88 us (5%)
    pallas_call x1, Pallas kernels, local(): pl.pallas_call(kernel, out_shape=jax.ShapeDtypeStruct(tokens.shape, BF16)...  32.3 us
    unnamed x1, local copies, waits for them, and re-layouts  1.88 us

profile of v1, /device:TPU:1, one launch (start us, length us, event | category | flops | bytes accessed | tf_op | source)
XLA Modules:
  0.0 34.1 jit_solution(16921585070489008035)
XLA Ops:
  0.0 32.3 %ssm_layer.1 = bf16[128,2048]{1,0:T(8,128)(2,1)} custom-call(bf16[128,2048]{1,0:T(8,128)(2,1)} %tokens_h.1, f32[1,128]{1,0:T(1,128)} %bitcast.11, f32[1,2048]{1,0:T(1,128)} %bitcast.7, bf16[2048,1024]{1,0:T(8,128)(2,1)} %inw_h.1, bf16[2,2,64,16,64]{4,3,2,1,0:T(8,128)(2,1)} %bitcast.6, f32[2,2,64,16,64]{4,3,2,1,0:T(8,128)} %sout_h.1, f32[2,64,64]{2,1,0:T(8,128)} %rate_h.1, ...), custom_call_target="tpu_custom_call" | custom-call | tf_op jit(solution)/shard_map/ssm_layer/pallas_call | solution.py:588
  32.3 1.9 %copy.15 = bf16[128,2048]{1,0:T(8,128)(2,1)} copy(bf16[128,2048]{1,0:T(8,128)(2,1)} %ssm_layer.1) | data formatting | bytes 1048576

commit v2 on v1

--- a/solution.py
+++ b/solution.py
@@ -62,17 +62,17 @@
 
 
 def kernel(
-    tokens_h, elapsed_h, ngain_h, inw_h, sin_h, sout_h, rate_h, angle_h, skip_h, glu_h, gbias_h, outw_h, ogain_h,
-    out_ref,
-    tokens_v, elapsed_v, ngain_v, inw_v, sin_v, sout_v, rate_v, angle_v, skip_v, glu_v, gbias_v, outw_v, ogain_v,
-    normed, acc, drv, resp, bst, cst, proj, dec, tabs, by_token, at_node, cell_decay, cell_gain, gain, states, spans, loc, ssum, lead, fade,
+    tokens_h, elapsed_h, ngain_h, inw_h, sin_h, sout_h, rate_h, angle_h, skip_h, glu_h, outw_h,
+    resp, glu_v, outw_v,
+    tokens_v, elapsed_v, ngain_v, inw_v, sin_v, sout_v, rate_v, angle_v, skip_v,
+    normed, acc, drv, bst, cst, proj, dec, tabs, by_token, at_node, cell_decay, cell_gain, gain, states, spans, loc, ssum, lead, fade,
     t_dev, t_line, g_in, x_in, x_far, e_new, e_fade, e_in,
     dma_sem, t_send, t_recv, u_send, u_recv, g_send, g_recv, x_send, x_recv, e_send, e_recv,
 ):
     sp = lax.axis_index("sp")
     tp = lax.axis_index("tp")
     yi, core = tp // 2, tp % 2
-    way = 1 - core
+    way = core
 
     def line_peer(k):
         return {"sp": sp, "tp": k}
@@ -94,11 +94,10 @@
 
     pairs = [
         (elapsed_h, elapsed_v), (tokens_h, tokens_v), (ngain_h, ngain_v), (rate_h, rate_v), (angle_h, angle_v),
-        (sin_h, sin_v), (sout_h, sout_v), (skip_h, skip_v), (gbias_h, gbias_v), (glu_h, glu_v),
-        (ogain_h, ogain_v), (outw_h, outw_v),
+        (sin_h, sin_v), (sout_h, sout_v), (skip_h, skip_v), (glu_h, glu_v), (outw_h, outw_v),
     ]
     copies = [pltpu.make_async_copy(a, b, dma_sem.at[k]) for k, (a, b) in enumerate(pairs)]
-    c_el, c_tok, c_ng, c_rate, c_ang, c_sin, c_sout, c_skip, c_gb, c_glu, c_og, c_ow = copies
+    c_el, c_tok, c_ng, c_rate, c_ang, c_sin, c_sout, c_skip, c_glu, c_ow = copies
     in_copies = [
         pltpu.make_async_copy(inw_h.at[pl.ds(k * 512, 512), :], inw_v.at[pl.ds(k * 512, 512), :], dma_sem.at[12 + k])
         for k in range(4)
@@ -107,7 +106,7 @@
         c.start()
     for c in in_copies:
         c.start()
-    for c in (c_sin, c_sout, c_skip, c_gb, c_glu, c_og, c_ow):
+    for c in (c_sin, c_sout, c_skip, c_glu, c_ow):
         c.start()
 
     barrier = pltpu.get_barrier_semaphore()
@@ -146,7 +145,6 @@
     row_i = lax.broadcasted_iota(jnp.int32, (ROWS, ROWS), 0)
     col_i = lax.broadcasted_iota(jnp.int32, (ROWS, ROWS), 1)
     order = jnp.where(col_i == (row_i % SUBS) * STEPS + row_i // SUBS, 1.0, 0.0).astype(BF16)
-    back = jnp.where(row_i == (col_i % SUBS) * STEPS + col_i // SUBS, 1.0, 0.0).astype(BF16)
     across = (((1,), (1,)), ((), ()))
     for k, rows in enumerate((token_rows, gain_rows)):
         by_token[k] = lax.dot_general(order, rows, across, preferred_element_type=F32).astype(BF16)
@@ -186,7 +184,7 @@
         return remote(x_in.at[peer], x_in.at[peer], x_send.at[k], x_recv.at[peer], plane_peer(peer))
 
     def g_out(d, q):
-        return remote(ssum.at[d, q], g_in.at[tp], g_send.at[q * 2 + d], g_recv.at[tp], line_peer(q * 2 + 1 - d))
+        return remote(ssum.at[d, q], g_in.at[tp], g_send.at[q * 2 + d], g_recv.at[tp], line_peer(q * 2 + d))
 
     def g_arr(k):
         peer = lax.rem(tp + k, LINE)
@@ -249,10 +247,6 @@
         resp[m, :, 128:256] = high_d * skip_v[:, 512 + m * 128:512 + (m + 1) * 128]
         drv[m, :, 0:128] = low_d.astype(BF16)
         drv[m, :, 128:256] = high_d.astype(BF16)
-
-    pl.semaphore_wait(barrier, LINE - 1 + LINES - 1)
-    for k in range(1, LINE):
-        t_out(k).start()
 
     c_sin.wait()
     nothing = jnp.zeros((128, 64), BF16)
@@ -322,17 +316,16 @@
                 ssum[d, q, 0, t:t + 1, :] = jnp.sum(m_re, axis=0, keepdims=True)
                 ssum[d, q, 1, t:t + 1, :] = jnp.sum(m_im, axis=0, keepdims=True)
 
-        @pl.when(q == 2)
+        @pl.when(q == 1)
         def _():
+            pl.semaphore_wait(barrier, LINE - 1 + LINES - 1)
             for k in range(1, LINE):
-                t_in(k).wait_recv()
-            total = t_dev[0]
-            for k in range(1, LINE):
-                total = total + t_dev[k]
-            t_line[sp] = total
-            for k in range(1, LINES):
-                peer, there = ahead(k)
-                pl.when(there)(u_out(k, peer).start)
+                t_out(k).start()
+
+        @pl.when(q > 0)
+        def _():
+            for d in range(2):
+                pl.when(tp != (q - 1) * 2 + d)(g_out(d, q - 1).start)
 
         values_at_nodes(0)
         products(0)
@@ -343,11 +336,11 @@
             if t + 2 < QUARTER:
                 values_at_nodes(t + 2)
             scan(t)
-        for d in range(2):
-            pl.when(tp != q * 2 + 1 - d)(g_out(d, q).start)
         return carry
 
     lax.fori_loop(0, TILES // QUARTER, first_pass, 0)
+    for d in range(2):
+        pl.when(tp != LINE - 2 + d)(g_out(d, TILES // QUARTER - 1).start)
 
     def lead_in(tile, carry):
         for d in range(2):
@@ -378,6 +371,16 @@
 
     lax.fori_loop(0, TILES, lead_in, 0)
 
+    for k in range(1, LINE):
+        t_in(k).wait_recv()
+    total = t_dev[0]
+    for k in range(1, LINE):
+        total = total + t_dev[k]
+    t_line[sp] = total
+    for k in range(1, LINES):
+        peer, there = ahead(k)
+        pl.when(there)(u_out(k, peer).start)
+
     c_sout.wait()
     lane_group = lax.broadcasted_iota(jnp.int32, (64, 128), 1) // 16
     blank = jnp.zeros((64, 128), BF16)
@@ -400,9 +403,6 @@
     lax.fori_loop(0, 4, spread, 0)
 
     g_in[tp] = ssum[way, yi]
-    for k in range(1, LINES):
-        peer, there = behind(k)
-        pl.when(there)(u_in(k, peer).wait_recv)
     places = [jnp.where(way == 0, o, LINE - 1 - o) for o in range(LINE)]
     gains = [quarter_decay(t_dev[k]) for k in places]
     for k in range(1, LINE):
@@ -425,14 +425,6 @@
         e_new[k, 1] = before[o][1]
         e_fade[k, 0] = before_d[o][0]
         e_fade[k, 1] = before_d[o][1]
-    between = jnp.zeros((SUBS, 128), F32)
-    for k in range(1, LINES):
-        peer, there = behind(k)
-        far_re, far_im = quarter_decay(between)
-        x_far[k, 0] = far_re
-        x_far[k, 1] = far_im
-        between = between + jnp.where(there, t_line[peer], 0.0)
-
     def local_pass(q, carry):
         total = resp[q]
         for t in range(QUARTER):
@@ -466,6 +458,17 @@
 
     lax.fori_loop(0, TILES // QUARTER, local_pass, 0)
 
+    for k in range(1, LINES):
+        peer, there = behind(k)
+        pl.when(there)(u_in(k, peer).wait_recv)
+    between = jnp.zeros((SUBS, 128), F32)
+    for k in range(1, LINES):
+        peer, there = behind(k)
+        far_re, far_im = quarter_decay(between)
+        x_far[k, 0] = far_re
+        x_far[k, 1] = far_im
+        between = between + jnp.where(there, t_line[peer], 0.0)
+
     gone = (zero, zero)
     for k in range(1, LINES):
         peer, there = behind(k)
@@ -488,8 +491,8 @@
             tile = q * QUARTER + t
             for d in range(2):
                 base = d * 256
-                e_re = jnp.broadcast_to(e_in[q * 2 + 1 - d, 0, t:t + 1, :], (16, 128))
-                e_im = jnp.broadcast_to(e_in[q * 2 + 1 - d, 1, t:t + 1, :], (16, 128))
+                e_re = jnp.broadcast_to(e_in[q * 2 + d, 0, t:t + 1, :], (16, 128))
+                e_im = jnp.broadcast_to(e_in[q * 2 + d, 1, t:t + 1, :], (16, 128))
                 for r in range(0, ROWS, 16):
                     f_re, f_im = dec[tile, r:r + 16, base:base + 128], dec[tile, r:r + 16, base + 128:base + 256]
                     m_re, m_im = times(f_re, f_im, e_re, e_im)
@@ -502,21 +505,36 @@
 
     lax.fori_loop(0, TILES // QUARTER, second_pass, 0)
 
-    c_gb.wait()
     c_glu.wait()
+    c_ow.wait()
+
+    for k in range(1, LINE):
+        t_out(k).wait_send()
+        e_out(k).wait_send()
+    for q in range(TILES // QUARTER):
+        for d in range(2):
+            pl.when(tp != q * 2 + d)(g_out(d, q).wait_send)
+    for k in range(1, LINES):
+        peer, there = ahead(k)
+        pl.when(there)(u_out(k, peer).wait_send)
+        pl.when(there)(x_out(k, peer).wait_send)
+
+
+def output_unit(resp, glu_v, outw_v, gbias_v, ogain_v, out_ref):
+    row_i = lax.broadcasted_iota(jnp.int32, (ROWS, ROWS), 0)
+    col_i = lax.broadcasted_iota(jnp.int32, (ROWS, ROWS), 1)
+    back = jnp.where(row_i == (col_i % SUBS) * STEPS + col_i // SUBS, 1.0, 0.0).astype(BF16)
     response = jnp.concatenate(
         [resp[m, :, 0:128] for m in range(4)] + [resp[m, :, 128:256] for m in range(4)], axis=1
     )
-    acc[...] = jax.nn.gelu(response, approximate=True)
-    active_low = acc[...].astype(BF16)
+    active = jax.nn.gelu(response, approximate=True)
+    active_low = active.astype(BF16)
     gates = []
     for n in range(4):
         at = slice(n * 256, (n + 1) * 256)
         gate = jnp.dot(active_low, glu_v[:, at], preferred_element_type=F32) + gbias_v[:, at]
-        gates.append((acc[:, at] * jax.nn.sigmoid(gate)).astype(BF16))
+        gates.append((active[:, at] * jax.nn.sigmoid(gate)).astype(BF16))
     gated = jnp.dot(back, jnp.concatenate(gates, axis=1), preferred_element_type=F32).astype(BF16)
-    c_og.wait()
-    c_ow.wait()
     outs, square = [], None
     for n in range(8):
         at = slice(n * 256, (n + 1) * 256)
@@ -529,17 +547,6 @@
         at = slice(n * 256, (n + 1) * 256)
         out_ref[:, at] = (outs[n] * scale * ogain_v[:, at]).astype(BF16)
 
-    for k in range(1, LINE):
-        t_out(k).wait_send()
-        e_out(k).wait_send()
-    for q in range(TILES // QUARTER):
-        for d in range(2):
-            pl.when(tp != q * 2 + 1 - d)(g_out(d, q).wait_send)
-    for k in range(1, LINES):
-        peer, there = ahead(k)
-        pl.when(there)(u_out(k, peer).wait_send)
-        pl.when(there)(x_out(k, peer).wait_send)
-
 
 def local(
     tokens, elapsed, norm_gain, in_weight, state_input, state_output, forget_rate, decay_angle,
@@ -547,16 +554,14 @@
 ):
     args = (
         tokens, elapsed.reshape(1, -1), norm_gain.reshape(1, -1), in_weight, state_input.transpose(0, 1, 2, 4, 3),
-        state_output, forget_rate, decay_angle, skip_gain.reshape(1, -1), glu_weight, glu_bias.reshape(1, -1),
-        out_weight, out_gain.reshape(1, -1),
+        state_output, forget_rate, decay_angle, skip_gain.reshape(1, -1), glu_weight, out_weight,
     )
     vm = pltpu.VMEM
-    scratch = [vm(a.shape, a.dtype) for a in args]
+    scratch = [vm(a.shape, a.dtype) for a in args[:9]]
     scratch += [
         vm((ROWS, 2048), BF16),
         vm((ROWS, 1024), F32),
         vm((4, ROWS, 256), BF16),
-        vm((4, ROWS, 256), F32),
         vm((4, 256, 512), BF16),
         vm((TILES, 512, 256), BF16),
         vm((TILES, ROWS, 512), F32),
@@ -585,17 +590,30 @@
     ]
     for count in (LINE, LINES, LINE, LINES, LINE):
         scratch += [pltpu.SemaphoreType.DMA((count,)), pltpu.SemaphoreType.DMA((count,))]
-    return pl.pallas_call(
+    inner = pl.BlockSpec(memory_space=pltpu.VMEM)
+    response, glu_held, out_held = pl.pallas_call(
         kernel,
-        out_shape=jax.ShapeDtypeStruct(tokens.shape, BF16),
-        in_specs=[pl.BlockSpec(memory_space=pl.ANY)] * len(args),
-        out_specs=pl.BlockSpec(memory_space=pltpu.VMEM),
+        out_shape=(
+            vm((4, ROWS, 256), F32),
+            vm(glu_weight.shape, BF16),
+            vm(out_weight.shape, BF16),
+        ),
+        in_specs=[pl.BlockSpec(memory_space=pltpu.HBM)] * len(args),
+        out_specs=(inner, inner, inner),
         scratch_shapes=scratch,
         compiler_params=pltpu.CompilerParams(
-            collective_id=0, has_side_effects=True, vmem_limit_bytes=67000000
+            collective_id=0, has_side_effects=True, vmem_limit_bytes=50000000
         ),
         name="ssm_layer",
     )(*args)
+    return pl.pallas_call(
+        output_unit,
+        out_shape=jax.ShapeDtypeStruct(tokens.shape, BF16),
+        in_specs=[inner] * 5,
+        out_specs=inner,
+        compiler_params=pltpu.CompilerParams(vmem_limit_bytes=16000000),
+        name="output_unit",
+    )(response, glu_held, out_held, glu_bias.reshape(1, -1), out_gain.reshape(1, -1))
 
 
 def solution(mesh):

time: 34.3 us -> 29.5 us (0.86)
  Pallas kernels: 32.3 us -> 29.4 us
  local copies, waits for them, and re-layouts: 1.88 us -> 0.01 us
    pallas_call x1 -> x2, Pallas kernels: 32.3 us -> 29.4 us  [the longest x1 27.2 us: local(): pl.pallas_call(kernel, out_shape=(vm((4, ROWS, 256), F32), vm(glu_weight....]
    unnamed x1 -> x4, local copies, waits for them, and re-layouts: 1.88 us -> 0.01 us
where the time goes in v2:
time: 29.5 us; the launch traced here: 29.4 us
  Pallas kernels  29.4 us (100%)
    pallas_call x1, Pallas kernels, local(): pl.pallas_call(kernel, out_shape=(vm((4, ROWS, 256), F32), vm(glu_weight....  27.2 us
    pallas_call x1, Pallas kernels, local(): pl.pallas_call(output_unit, out_shape=jax.ShapeDtypeStruct(tokens.shape,...  2.23 us

profile of v2, /device:TPU:1, one launch (start us, length us, event | category | flops | bytes accessed | tf_op | source)
XLA Modules:
  0.0 29.4 jit_solution(3329800146369675433)
XLA Ops:
  0.0 0.0 copy-start
  0.0 0.0 copy-start.1
  0.0 27.2 %ssm_layer.1 = (f32[4,128,256]{2,1,0:T(8,128)S(1)}, bf16[1024,1024]{1,0:T(8,128)(2,1)S(1)}, bf16[1024,2048]{1,0:T(8,128)(2,1)S(1)}) custom-call(bf16[128,2048]{1,0:T(8,128)(2,1)} %tokens_h.1, f32[1,128]{1,0:T(1,128)} %bitcast.11, f32[1,2048]{1,0:T(1,128)} %bitcast.9, bf16[2048,1024]{1,0:T(8,128)(2,1)} %inw_h.1, bf16[2,2,64,16,64]{4,3,2,1,0:T(8,128)(2,1)} %bitcast.8, ...), custom_call_target="tpu_custom_call" | custom-call | tf_op jit(solution)/shard_map/ssm_layer/pallas_call | solution.py:594
  27.2 0.0 copy-done
  27.2 0.0 copy-done.1
  27.2 2.2 %output_unit.1 = bf16[128,2048]{1,0:T(8,128)(2,1)} custom-call(f32[4,128,256]{2,1,0:T(8,128)S(1)} %get-tuple-element.8.resp, bf16[1024,1024]{1,0:T(8,128)(2,1)S(1)} %get-tuple-element.9.glu_v, bf16[1024,2048]{1,0:T(8,128)(2,1)S(1)} %get-tuple-element.10.outw_v, f32[1,1024]{1,0:T(1,128)S(1)} %bitcast.7, f32[1,2048]{1,0:T(1,128)S(1)} %bitcast.6), custom_call_target="tpu_custom_call" | custom-call | tf_op jit(solution)/shard_map/output_unit/pallas_call | solution.py:609
Async XLA Ops:
  0.0 27.2 %copy-start = (f32[2048]{0:T(1024)S(1)}, f32[2048]{0:T(1024)}, u32[]{:S(2)}) copy-start(f32[2048]{0:T(1024)} %param.25) | copy-start | bytes 24580
  0.0 27.2 %copy-start.1 = (f32[1024]{0:T(1024)S(1)}, f32[1024]{0:T(1024)}, u32[]{:S(2)}) copy-start(f32[1024]{0:T(1024)} %param.23) | copy-start | bytes 12292

commit v3 on v2

--- a/solution.py
+++ b/solution.py
@@ -153,10 +153,11 @@
     for k in range(1, 16):
         nodes = jnp.where(node_i == k, POINTS[k], nodes)
     at_node[...] = nodes
-    none32 = jnp.zeros((32, 512), BF16)
+    none32 = jnp.zeros((32, 256), BF16)
     none80 = jnp.zeros((80, 256), BF16)
     for t in range(QUARTER):
         cell_decay[t, 96:128, :] = none32
+    for t in range(QUARTER // 2):
         cell_gain[t, 48:128, :] = none80
     stretch = lane8 // STEPS
     for k, mask in enumerate((stretch == sub8, stretch > sub8, stretch < sub8)):
@@ -193,10 +194,6 @@
     def e_out(k):
         peer = lax.rem(tp + k, LINE)
         return remote(e_new.at[peer], e_in.at[tp], e_send.at[k], e_recv.at[tp], line_peer(peer))
-
-    def e_arr(k):
-        peer = lax.rem(tp + k, LINE)
-        return remote(e_new.at[peer], e_in.at[peer], e_send.at[k], e_recv.at[peer], line_peer(peer))
 
     c_rate.wait()
     c_ang.wait()
@@ -261,86 +258,97 @@
 
     group_lane = (lax.broadcasted_iota(jnp.int32, (ROWS, 256), 1) // 16) % 8
 
-    def first_pass(q, carry):
+    def first_pass(d, q):
+        base = d * 256
+
         def values_at_nodes(t):
             row = pl.ds(q * QUARTER + t, 1)
             x = at_node[...]
-            for d in range(2):
-                rate2, double, both = [jnp.broadcast_to(tabs[d, k, row, :], (16, 128)) for k in (0, 1, 4)]
-                size = jnp.exp2(rate2 * x)
-                y = double * x
-                near = y * horner(y, (1.0, -0.5, 1.0 / 6.0, -1.0 / 24.0))
-                gap = jnp.where(y < 0.03, near, 1.0 - size * size)
-                for part, value in enumerate(decay_parts(size, both * x)):
-                    v1, v2, v3 = in_parts(value, 3)
-                    at = slice((d * 2 + part) * 128, (d * 2 + part + 1) * 128)
-                    for k, v in enumerate((v1, v2, v1, v2, v3, v1)):
-                        cell_decay[t, k * 16:(k + 1) * 16, at] = v
-                g1, g2 = in_parts(gap * lax.rsqrt(jnp.maximum(gap * x, 1e-37)), 2)
-                for k, v in enumerate((g1, g2, g1)):
-                    cell_gain[t, k * 16:(k + 1) * 16, d * 128:(d + 1) * 128] = v
+            rate2, double, both = [jnp.broadcast_to(tabs[d, k, row, :], (16, 128)) for k in (0, 1, 4)]
+            size = jnp.exp2(rate2 * x)
+            y = double * x
+            near = y * horner(y, (1.0, -0.5, 1.0 / 6.0, -1.0 / 24.0))
+            gap = jnp.where(y < 0.03, near, 1.0 - size * size)
+            for part, value in enumerate(decay_parts(size, both * x)):
+                v1, v2, v3 = in_parts(value, 3)
+                for k, v in enumerate((v1, v2, v1, v2, v3, v1)):
+                    cell_decay[t, k * 16:(k + 1) * 16, part * 128:(part + 1) * 128] = v
+            g1, g2 = in_parts(gap * lax.rsqrt(jnp.maximum(gap * x, 1e-37)), 2)
+            at = slice(t % 2 * 128, t % 2 * 128 + 128)
+            for k, v in enumerate((g1, g2, g1)):
+                cell_gain[t // 2, k * 16:(k + 1) * 16, at] = v
 
         def products(t):
-            tile = q * QUARTER + t
-            dec[tile] = jnp.dot(by_token[0], cell_decay[t], preferred_element_type=F32)
-            gain[t] = jnp.dot(by_token[1], cell_gain[t], preferred_element_type=F32)
-            lhs = drv[q] * jnp.where(group_lane == t, 1.0, 0.0).astype(BF16)
-            proj[tile] = jnp.dot(lhs, bst[q], preferred_element_type=F32)
+            gain[t // 2] = jnp.dot(by_token[1], cell_gain[t // 2], preferred_element_type=F32)
+            for u in (t, t + 1):
+                tile = q * QUARTER + u
+                dec[tile, :, base:base + 256] = jnp.dot(by_token[0], cell_decay[u], preferred_element_type=F32)
+                lhs = drv[q] * jnp.where(group_lane == u, 1.0, 0.0).astype(BF16)
+                proj[tile, :, base:base + 256] = jnp.dot(
+                    lhs, bst[q, :, base:base + 256], preferred_element_type=F32
+                )
 
         def scan(t):
             tile = q * QUARTER + t
-            for d in range(2):
-                s_re = s_im = None
-                base = d * 256
-                for j in range(STEPS) if d == 0 else range(STEPS - 1, -1, -1):
-                    at = pl.ds(j * SUBS, SUBS)
-                    damp = gain[t, at, d * 128:(d + 1) * 128]
-                    p_re = proj[tile, at, base:base + 128] * damp
-                    p_im = proj[tile, at, base + 128:base + 256] * damp
-                    proj[tile, at, base:base + 128] = p_re
-                    proj[tile, at, base + 128:base + 256] = p_im
-                    if s_re is None:
-                        s_re, s_im = p_re, p_im
-                    else:
-                        a_re, a_im = dec[tile, at, base:base + 128], dec[tile, at, base + 128:base + 256]
-                        n_re, n_im = times(a_re, a_im, s_re, s_im)
-                        s_re, s_im = n_re + p_re, n_im + p_im
-                loc[tile, d, 0] = s_re
-                loc[tile, d, 1] = s_im
-                k = 2 if d == 0 else 4
-                rate2, high, low, both = [
-                    jnp.broadcast_to(tabs[d, i, pl.ds(tile, 1), :], (SUBS, 128)) for i in (0, 2, 3, 4)
-                ]
-                w_re, w_im = stretch_decay(rate2, high, low, both, spans[k], spans[k + 1])
-                m_re, m_im = times(w_re, w_im, s_re, s_im)
-                ssum[d, q, 0, t:t + 1, :] = jnp.sum(m_re, axis=0, keepdims=True)
-                ssum[d, q, 1, t:t + 1, :] = jnp.sum(m_im, axis=0, keepdims=True)
-
-        @pl.when(q == 1)
+            s_re = s_im = None
+            for j in range(STEPS) if d == 0 else range(STEPS - 1, -1, -1):
+                at = pl.ds(j * SUBS, SUBS)
+                damp = gain[t // 2, at, t % 2 * 128:t % 2 * 128 + 128]
+                p_re = proj[tile, at, base:base + 128] * damp
+                p_im = proj[tile, at, base + 128:base + 256] * damp
+                proj[tile, at, base:base + 128] = p_re
+                proj[tile, at, base + 128:base + 256] = p_im
+                if s_re is None:
+                    s_re, s_im = p_re, p_im
+                else:
+                    a_re, a_im = dec[tile, at, base:base + 128], dec[tile, at, base + 128:base + 256]
+                    n_re, n_im = times(a_re, a_im, s_re, s_im)
+                    s_re, s_im = n_re + p_re, n_im + p_im
+            loc[tile, d, 0] = s_re
+            loc[tile, d, 1] = s_im
+            k = 2 if d == 0 else 4
+            rate2, high, low, both = [
+                jnp.broadcast_to(tabs[d, i, pl.ds(tile, 1), :], (SUBS, 128)) for i in (0, 2, 3, 4)
+            ]
+            w_re, w_im = stretch_decay(rate2, high, low, both, spans[k], spans[k + 1])
+            m_re, m_im = times(w_re, w_im, s_re, s_im)
+            ssum[d, q, 0, t:t + 1, :] = jnp.sum(m_re, axis=0, keepdims=True)
+            ssum[d, q, 1, t:t + 1, :] = jnp.sum(m_im, axis=0, keepdims=True)
+
+        for t in (0, 1):
+            values_at_nodes(t)
+        products(0)
+        for t in (2, 3):
+            values_at_nodes(t)
+        for t in range(0, QUARTER, 2):
+            if t + 2 < QUARTER:
+                products(t + 2)
+            for u in (t, t + 1):
+                if u + 4 < QUARTER:
+                    values_at_nodes(u + 4)
+                scan(u)
+
+    def backward_quarter(q, carry):
+        @pl.when(q == 2)
         def _():
             pl.semaphore_wait(barrier, LINE - 1 + LINES - 1)
             for k in range(1, LINE):
                 t_out(k).start()
-
-        @pl.when(q > 0)
-        def _():
-            for d in range(2):
-                pl.when(tp != (q - 1) * 2 + d)(g_out(d, q - 1).start)
-
-        values_at_nodes(0)
-        products(0)
-        values_at_nodes(1)
-        for t in range(QUARTER):
-            if t + 1 < QUARTER:
-                products(t + 1)
-            if t + 2 < QUARTER:
-                values_at_nodes(t + 2)
-            scan(t)
+            pl.when(tp != 1)(g_out(1, 0).start)
+
+        pl.when(jnp.logical_and(q >= 2, tp != q * 2 - 1))(g_out(1, q - 1).start)
+
+        first_pass(1, q)
         return carry
 
-    lax.fori_loop(0, TILES // QUARTER, first_pass, 0)
-    for d in range(2):
-        pl.when(tp != LINE - 2 + d)(g_out(d, TILES // QUARTER - 1).start)
+    def forward_quarter(q, carry):
+        first_pass(0, q)
+        pl.when(tp != q * 2)(g_out(0, q).start)
+        return carry
+
+    lax.fori_loop(0, TILES // QUARTER, backward_quarter, 0)
+    pl.when(tp != LINE - 1)(g_out(1, TILES // QUARTER - 1).start)
+    lax.fori_loop(0, TILES // QUARTER, forward_quarter, 0)
 
     def lead_in(tile, carry):
         for d in range(2):
@@ -369,19 +377,6 @@
             fade[tile, d, 1] = g_im
         return carry
 
-    lax.fori_loop(0, TILES, lead_in, 0)
-
-    for k in range(1, LINE):
-        t_in(k).wait_recv()
-    total = t_dev[0]
-    for k in range(1, LINE):
-        total = total + t_dev[k]
-    t_line[sp] = total
-    for k in range(1, LINES):
-        peer, there = ahead(k)
-        pl.when(there)(u_out(k, peer).start)
-
-    c_sout.wait()
     lane_group = lax.broadcasted_iota(jnp.int32, (64, 128), 1) // 16
     blank = jnp.zeros((64, 128), BF16)
 
@@ -400,7 +395,29 @@
                     cst[tile, at + 64:at + 128, 128:256] = jnp.where(lane_group == i, upper, 0.0).astype(BF16)
         return carry
 
-    lax.fori_loop(0, 4, spread, 0)
+
+    def own_work():
+        lax.fori_loop(0, TILES, lead_in, 0)
+        lax.fori_loop(0, 4, spread, 0)
+
+    def pass_on_elapsed():
+        for k in range(1, LINE):
+            t_in(k).wait_recv()
+        total = t_dev[0]
+        for k in range(1, LINE):
+            total = total + t_dev[k]
+        t_line[sp] = total
+        for k in range(1, LINES):
+            peer, there = ahead(k)
+            pl.when(there)(u_out(k, peer).start)
+
+    c_sout.wait()
+
+    @pl.when(core == 0)
+    def _():
+        own_work()
+
+    pass_on_elapsed()
 
     g_in[tp] = ssum[way, yi]
     places = [jnp.where(way == 0, o, LINE - 1 - o) for o in range(LINE)]
@@ -425,6 +442,10 @@
         e_new[k, 1] = before[o][1]
         e_fade[k, 0] = before_d[o][0]
         e_fade[k, 1] = before_d[o][1]
+    @pl.when(core == 1)
+    def _():
+        own_work()
+
     def local_pass(q, carry):
         total = resp[q]
         for t in range(QUARTER):
@@ -456,7 +477,7 @@
         resp[q] = total + jnp.dot(states[QUARTER - 1], cst[q * QUARTER + QUARTER - 1], preferred_element_type=F32)
         return carry
 
-    lax.fori_loop(0, TILES // QUARTER, local_pass, 0)
+    lax.fori_loop(0, 2, local_pass, 0)
 
     for k in range(1, LINES):
         peer, there = behind(k)
@@ -482,15 +503,16 @@
     for k in range(1, LINE):
         e_out(k).start()
     e_in[tp] = e_new[tp]
-    for k in range(1, LINE):
-        e_arr(k).wait_recv()
-
-    def second_pass(q, carry):
-        total = resp[q]
-        for t in range(QUARTER):
-            tile = q * QUARTER + t
-            for d in range(2):
-                base = d * 256
+    def second_pass(d):
+        base = d * 256
+        for chip in range(4):
+            k = chip * 2 + d
+            pl.when(tp != k)(remote(e_new.at[k], e_in.at[k], e_send.at[0], e_recv.at[k], line_peer(k)).wait_recv)
+
+        def quarter(q, carry):
+            total = resp[q]
+            for t in range(QUARTER):
+                tile = q * QUARTER + t
                 e_re = jnp.broadcast_to(e_in[q * 2 + d, 0, t:t + 1, :], (16, 128))
                 e_im = jnp.broadcast_to(e_in[q * 2 + d, 1, t:t + 1, :], (16, 128))
                 for r in range(0, ROWS, 16):
@@ -498,12 +520,18 @@
                     m_re, m_im = times(f_re, f_im, e_re, e_im)
                     states[t, r:r + 16, base:base + 128] = m_re.astype(BF16)
                     states[t, r:r + 16, base + 128:base + 256] = m_im.astype(BF16)
-            if t:
-                total = total + jnp.dot(states[t - 1], cst[tile - 1], preferred_element_type=F32)
-        resp[q] = total + jnp.dot(states[QUARTER - 1], cst[q * QUARTER + QUARTER - 1], preferred_element_type=F32)
-        return carry
-
-    lax.fori_loop(0, TILES // QUARTER, second_pass, 0)
+                total = total + jnp.dot(
+                    states[t, :, base:base + 256], cst[tile, base:base + 256, :], preferred_element_type=F32
+                )
+            resp[q] = total
+            return carry
+
+        for q in range(TILES // QUARTER):
+            quarter(q, 0)
+
+    lax.fori_loop(2, 4, local_pass, 0)
+    second_pass(0)
+    second_pass(1)
 
     c_glu.wait()
     c_ow.wait()
@@ -569,9 +597,9 @@
         vm((2, 5, TILES, 128), F32),
         vm((2, ROWS, 128), BF16),
         vm((16, 128), F32),
-        vm((QUARTER, 128, 512), BF16),
         vm((QUARTER, 128, 256), BF16),
-        vm((QUARTER, ROWS, 256), F32),
+        vm((QUARTER // 2, 128, 256), BF16),
+        vm((QUARTER // 2, ROWS, 256), F32),
         vm((QUARTER, ROWS, 512), BF16),
         vm((6, SUBS, 128), F32),
         vm((TILES, 2, 2, SUBS, 128), F32),

time: 29.5 us -> 27.1 us (0.919); the launches traced: 29.4 us -> 26.6 us
  Pallas kernels: 29.4 us -> 26.6 us
    pallas_call x1, Pallas kernels: 27.2 us -> 24.4 us  [local(): pl.pallas_call(kernel, out_shape=(vm((4, ROWS, 256), F32), vm(glu_weight....]
where the time goes in v3:
time: 27.1 us; the launch traced here: 26.6 us
  Pallas kernels  26.6 us (98%)
    pallas_call x1, Pallas kernels, local(): pl.pallas_call(kernel, out_shape=(vm((4, ROWS, 256), F32), vm(glu_weight....  24.4 us
    pallas_call x1, Pallas kernels, local(): pl.pallas_call(output_unit, out_shape=jax.ShapeDtypeStruct(tokens.shape,...  2.23 us

profile of v3, /device:TPU:1, one launch (start us, length us, event | category | flops | bytes accessed | tf_op | source)
XLA Modules:
  0.0 26.6 jit_solution(9574625105492016088)
XLA Ops:
  0.0 0.0 copy-start
  0.0 0.0 copy-start.1
  0.0 24.4 %ssm_layer.1 = (f32[4,128,256]{2,1,0:T(8,128)S(1)}, bf16[1024,1024]{1,0:T(8,128)(2,1)S(1)}, bf16[1024,2048]{1,0:T(8,128)(2,1)S(1)}) custom-call(bf16[128,2048]{1,0:T(8,128)(2,1)} %tokens_h.1, f32[1,128]{1,0:T(1,128)} %bitcast.11, f32[1,2048]{1,0:T(1,128)} %bitcast.9, bf16[2048,1024]{1,0:T(8,128)(2,1)} %inw_h.1, bf16[2,2,64,16,64]{4,3,2,1,0:T(8,128)(2,1)} %bitcast.8, ...), custom_call_target="tpu_custom_call" | custom-call | tf_op jit(solution)/shard_map/ssm_layer/pallas_call | solution.py:622
  24.4 0.0 copy-done
  24.4 0.0 copy-done.1
  24.4 2.2 %output_unit.1 = bf16[128,2048]{1,0:T(8,128)(2,1)} custom-call(f32[4,128,256]{2,1,0:T(8,128)S(1)} %get-tuple-element.8.resp, bf16[1024,1024]{1,0:T(8,128)(2,1)S(1)} %get-tuple-element.9.glu_v, bf16[1024,2048]{1,0:T(8,128)(2,1)S(1)} %get-tuple-element.10.outw_v, f32[1,1024]{1,0:T(1,128)S(1)} %bitcast.7, f32[1,2048]{1,0:T(1,128)S(1)} %bitcast.6), custom_call_target="tpu_custom_call" | custom-call | tf_op jit(solution)/shard_map/output_unit/pallas_call | solution.py:637
Async XLA Ops:
  0.0 24.4 %copy-start = (f32[2048]{0:T(1024)S(1)}, f32[2048]{0:T(1024)}, u32[]{:S(2)}) copy-start(f32[2048]{0:T(1024)} %param.25) | copy-start | bytes 24580
  0.0 24.4 %copy-start.1 = (f32[1024]{0:T(1024)S(1)}, f32[1024]{0:T(1024)}, u32[]{:S(2)}) copy-start(f32[1024]{0:T(1024)} %param.23) | copy-start | bytes 12292

commit v4 on v3

--- a/solution.py
+++ b/solution.py
@@ -99,7 +99,7 @@
     copies = [pltpu.make_async_copy(a, b, dma_sem.at[k]) for k, (a, b) in enumerate(pairs)]
     c_el, c_tok, c_ng, c_rate, c_ang, c_sin, c_sout, c_skip, c_glu, c_ow = copies
     in_copies = [
-        pltpu.make_async_copy(inw_h.at[pl.ds(k * 512, 512), :], inw_v.at[pl.ds(k * 512, 512), :], dma_sem.at[12 + k])
+        pltpu.make_async_copy(inw_h.at[pl.ds(k * 512, 512), :], inw_v.at[pl.ds(k * 512, 512), :], dma_sem.at[11 + k])
         for k in range(4)
     ]
     for c in (c_el, c_tok, c_ng, c_rate, c_ang):
@@ -165,35 +165,35 @@
         spans[2 * k + 1] = picked(mask, rest)
 
     def t_out(k):
-        peer = lax.rem(tp + k, LINE)
-        return remote(t_dev.at[tp], t_dev.at[tp], t_send.at[k], t_recv.at[tp], line_peer(peer))
-
-    def t_in(k):
-        peer = lax.rem(tp + k, LINE)
-        return remote(t_dev.at[peer], t_dev.at[peer], t_send.at[k], t_recv.at[peer], line_peer(peer))
-
-    def u_out(k, peer):
-        return remote(t_line.at[sp], t_line.at[sp], u_send.at[k], u_recv.at[sp], plane_peer(peer))
-
-    def u_in(k, peer):
-        return remote(t_line.at[peer], t_line.at[peer], u_send.at[k], u_recv.at[peer], plane_peer(peer))
-
-    def x_out(k, peer):
-        return remote(x_in.at[sp], x_in.at[sp], x_send.at[k], x_recv.at[sp], plane_peer(peer))
-
-    def x_arr(k, peer):
-        return remote(x_in.at[peer], x_in.at[peer], x_send.at[k], x_recv.at[peer], plane_peer(peer))
+        return remote(t_dev.at[tp], t_dev.at[tp], t_send.at[0], t_recv.at[0], line_peer(lax.rem(tp + k, LINE)))
+
+    def u_out(peer):
+        return remote(t_line.at[sp], t_line.at[sp], u_send.at[0], u_recv.at[0], plane_peer(peer))
+
+    def x_out(peer):
+        return remote(x_in.at[sp], x_in.at[sp], x_send.at[0], x_recv.at[0], plane_peer(peer))
 
     def g_out(d, q):
-        return remote(ssum.at[d, q], g_in.at[tp], g_send.at[q * 2 + d], g_recv.at[tp], line_peer(q * 2 + d))
-
-    def g_arr(k):
-        peer = lax.rem(tp + k, LINE)
-        return remote(ssum.at[0, 0], g_in.at[peer], g_send.at[k], g_recv.at[peer], line_peer(peer))
+        return remote(ssum.at[d, q], g_in.at[tp], g_send.at[0], g_recv.at[0], line_peer(q * 2 + d))
 
     def e_out(k):
         peer = lax.rem(tp + k, LINE)
-        return remote(e_new.at[peer], e_in.at[tp], e_send.at[k], e_recv.at[tp], line_peer(peer))
+        return remote(e_new.at[peer], e_in.at[tp], e_send.at[0], e_recv.at[core], line_peer(peer))
+
+    def blocks(buf, n, send_sem, recv_sem):
+        part = buf.at[pl.ds(0, n)]
+        return remote(part, part, send_sem, recv_sem, line_peer(lax.rem(tp + 1, LINE)))
+
+    lines_behind = jnp.where(way == 0, sp, LINES - 1 - sp)
+    lines_ahead = LINES - 1 - lines_behind
+
+    def lines_in(buf, send_sem, recv_sem):
+        for n in range(1, LINES):
+            pl.when(lines_behind == n)(blocks(buf, n, send_sem, recv_sem).wait_recv)
+
+    def lines_out(buf, send_sem, recv_sem):
+        for n in range(1, LINES):
+            pl.when(lines_ahead == n)(blocks(buf, n, send_sem, recv_sem).wait_send)
 
     c_rate.wait()
     c_ang.wait()
@@ -401,15 +401,14 @@
         lax.fori_loop(0, 4, spread, 0)
 
     def pass_on_elapsed():
-        for k in range(1, LINE):
-            t_in(k).wait_recv()
+        blocks(t_dev, LINE - 1, t_send.at[0], t_recv.at[0]).wait_recv()
         total = t_dev[0]
         for k in range(1, LINE):
             total = total + t_dev[k]
         t_line[sp] = total
         for k in range(1, LINES):
             peer, there = ahead(k)
-            pl.when(there)(u_out(k, peer).start)
+            pl.when(there)(u_out(peer).start)
 
     c_sout.wait()
 
@@ -422,8 +421,7 @@
     g_in[tp] = ssum[way, yi]
     places = [jnp.where(way == 0, o, LINE - 1 - o) for o in range(LINE)]
     gains = [quarter_decay(t_dev[k]) for k in places]
-    for k in range(1, LINE):
-        g_arr(k).wait_recv()
+    blocks(g_in, LINE - 1, g_send.at[0], g_recv.at[0]).wait_recv()
     zero, one = jnp.zeros((QUARTER, 128), F32), jnp.ones((QUARTER, 128), F32)
     run, run_d, before, before_d = (zero, zero), (one, zero), [], []
     for o, k in enumerate(places):
@@ -436,7 +434,7 @@
     x_in[sp, 1] = run[1]
     for k in range(1, LINES):
         peer, there = ahead(k)
-        pl.when(there)(x_out(k, peer).start)
+        pl.when(there)(x_out(peer).start)
     for o, k in enumerate(places):
         e_new[k, 0] = before[o][0]
         e_new[k, 1] = before[o][1]
@@ -479,9 +477,11 @@
 
     lax.fori_loop(0, 2, local_pass, 0)
 
-    for k in range(1, LINES):
-        peer, there = behind(k)
-        pl.when(there)(u_in(k, peer).wait_recv)
+    blocks(t_dev, LINE - 1, t_send.at[0], t_recv.at[0]).wait_send()
+    blocks(g_in, LINE - 1, g_send.at[0], g_recv.at[0]).wait_send()
+    lines_out(t_line, u_send.at[0], u_recv.at[0])
+
+    lines_in(t_line, u_send.at[0], u_recv.at[0])
     between = jnp.zeros((SUBS, 128), F32)
     for k in range(1, LINES):
         peer, there = behind(k)
@@ -490,10 +490,10 @@
         x_far[k, 1] = far_im
         between = between + jnp.where(there, t_line[peer], 0.0)
 
+    lines_in(x_in, x_send.at[0], x_recv.at[0])
     gone = (zero, zero)
     for k in range(1, LINES):
         peer, there = behind(k)
-        pl.when(there)(x_arr(k, peer).wait_recv)
         moved = times(x_far[k, 0], x_far[k, 1], x_in[peer, 0], x_in[peer, 1])
         gone = tuple(g + jnp.where(there, m, 0.0) for g, m in zip(gone, moved))
     for k in range(LINE):
@@ -505,9 +505,8 @@
     e_in[tp] = e_new[tp]
     def second_pass(d):
         base = d * 256
-        for chip in range(4):
-            k = chip * 2 + d
-            pl.when(tp != k)(remote(e_new.at[k], e_in.at[k], e_send.at[0], e_recv.at[k], line_peer(k)).wait_recv)
+        for n in (3, 4):
+            pl.when((core == d) == (n == 3))(blocks(e_in, n, e_send.at[0], e_recv.at[d]).wait_recv)
 
         def quarter(q, carry):
             total = resp[q]
@@ -530,22 +529,14 @@
             quarter(q, 0)
 
     lax.fori_loop(2, 4, local_pass, 0)
+    lines_out(x_in, x_send.at[0], x_recv.at[0])
     second_pass(0)
     second_pass(1)
 
     c_glu.wait()
     c_ow.wait()
 
-    for k in range(1, LINE):
-        t_out(k).wait_send()
-        e_out(k).wait_send()
-    for q in range(TILES // QUARTER):
-        for d in range(2):
-            pl.when(tp != q * 2 + d)(g_out(d, q).wait_send)
-    for k in range(1, LINES):
-        peer, there = ahead(k)
-        pl.when(there)(u_out(k, peer).wait_send)
-        pl.when(there)(x_out(k, peer).wait_send)
+    blocks(e_in, LINE - 1, e_send.at[0], e_recv.at[0]).wait_send()
 
 
 def output_unit(resp, glu_v, outw_v, gbias_v, ogain_v, out_ref):
@@ -614,10 +605,9 @@
         vm((LINE, 2, QUARTER, 128), F32),
         vm((LINE, 2, QUARTER, 128), F32),
         vm((LINE, 2, QUARTER, 128), F32),
-        pltpu.SemaphoreType.DMA((16,)),
+        pltpu.SemaphoreType.DMA((15,)),
     ]
-    for count in (LINE, LINES, LINE, LINES, LINE):
-        scratch += [pltpu.SemaphoreType.DMA((count,)), pltpu.SemaphoreType.DMA((count,))]
+    scratch += [pltpu.SemaphoreType.DMA((n,)) for n in (1, 1, 1, 1, 1, 1, 1, 1, 1, 2)]
     inner = pl.BlockSpec(memory_space=pltpu.VMEM)
     response, glu_held, out_held = pl.pallas_call(
         kernel,

time: 27.1 us -> 26 us (0.959)
  Pallas kernels: 26.6 us -> 25.4 us
    pallas_call x1, Pallas kernels: 24.4 us -> 23.2 us  [local(): pl.pallas_call(kernel, out_shape=(vm((4, ROWS, 256), F32), vm(glu_weight....]
where the time goes in v4:
time: 26 us; the launch traced here: 25.5 us
  Pallas kernels  25.4 us (98%)
    pallas_call x1, Pallas kernels, local(): pl.pallas_call(kernel, out_shape=(vm((4, ROWS, 256), F32), vm(glu_weight....  23.2 us
    pallas_call x1, Pallas kernels, local(): pl.pallas_call(output_unit, out_shape=jax.ShapeDtypeStruct(tokens.shape,...  2.23 us

profile of v4, /device:TPU:1, one launch (start us, length us, event | category | flops | bytes accessed | tf_op | source)
XLA Modules:
  0.0 25.5 jit_solution(9075041007632309819)
XLA Ops:
  0.0 0.0 copy-start
  0.0 0.0 copy-start.1
  0.0 23.2 %ssm_layer.1 = (f32[4,128,256]{2,1,0:T(8,128)S(1)}, bf16[1024,1024]{1,0:T(8,128)(2,1)S(1)}, bf16[1024,2048]{1,0:T(8,128)(2,1)S(1)}) custom-call(bf16[128,2048]{1,0:T(8,128)(2,1)} %tokens_h.1, f32[1,128]{1,0:T(1,128)} %bitcast.11, f32[1,2048]{1,0:T(1,128)} %bitcast.9, bf16[2048,1024]{1,0:T(8,128)(2,1)} %inw_h.1, bf16[2,2,64,16,64]{4,3,2,1,0:T(8,128)(2,1)} %bitcast.8, ...), custom_call_target="tpu_custom_call" | custom-call | tf_op jit(solution)/shard_map/ssm_layer/pallas_call | solution.py:612
  23.2 0.0 copy-done
  23.2 0.0 copy-done.1
  23.2 2.2 %output_unit.1 = bf16[128,2048]{1,0:T(8,128)(2,1)} custom-call(f32[4,128,256]{2,1,0:T(8,128)S(1)} %get-tuple-element.8.resp, bf16[1024,1024]{1,0:T(8,128)(2,1)S(1)} %get-tuple-element.9.glu_v, bf16[1024,2048]{1,0:T(8,128)(2,1)S(1)} %get-tuple-element.10.outw_v, f32[1,1024]{1,0:T(1,128)S(1)} %bitcast.7, f32[1,2048]{1,0:T(1,128)S(1)} %bitcast.6), custom_call_target="tpu_custom_call" | custom-call | tf_op jit(solution)/shard_map/output_unit/pallas_call | solution.py:627
Async XLA Ops:
  0.0 23.2 %copy-start = (f32[2048]{0:T(1024)S(1)}, f32[2048]{0:T(1024)}, u32[]{:S(2)}) copy-start(f32[2048]{0:T(1024)} %param.25) | copy-start | bytes 24580
  0.0 23.2 %copy-start.1 = (f32[1024]{0:T(1024)S(1)}, f32[1024]{0:T(1024)}, u32[]{:S(2)}) copy-start(f32[1024]{0:T(1024)} %param.23) | copy-start | bytes 12292

commit v5 on v4

--- a/solution.py
+++ b/solution.py
@@ -397,7 +397,12 @@
 
 
     def own_work():
-        lax.fori_loop(0, TILES, lead_in, 0)
+        def four(r, carry):
+            for t in range(4):
+                lead_in(r * 4 + t, carry)
+            return carry
+
+        lax.fori_loop(0, TILES // 4, four, 0)
         lax.fori_loop(0, 4, spread, 0)
 
     def pass_on_elapsed():
@@ -539,7 +544,7 @@
     blocks(e_in, LINE - 1, e_send.at[0], e_recv.at[0]).wait_send()
 
 
-def output_unit(resp, glu_v, outw_v, gbias_v, ogain_v, out_ref):
+def output_unit(resp, glu_v, outw_v, gbias_v, ogain_v, out_ref, held, sems):
     row_i = lax.broadcasted_iota(jnp.int32, (ROWS, ROWS), 0)
     col_i = lax.broadcasted_iota(jnp.int32, (ROWS, ROWS), 1)
     back = jnp.where(row_i == (col_i % SUBS) * STEPS + col_i // SUBS, 1.0, 0.0).astype(BF16)
@@ -562,9 +567,16 @@
         part = jnp.sum(piece * piece, axis=-1, keepdims=True)
         square = part if square is None else square + part
     scale = lax.rsqrt(square * (1.0 / 2048.0) + EPS)
-    for n in range(8):
-        at = slice(n * 256, (n + 1) * 256)
-        out_ref[:, at] = (outs[n] * scale * ogain_v[:, at]).astype(BF16)
+    sent = []
+    for r in range(0, ROWS, 32):
+        for n in range(8):
+            at = slice(n * 256, (n + 1) * 256)
+            held[r:r + 32, at] = (outs[n][r:r + 32] * scale[r:r + 32] * ogain_v[:, at]).astype(BF16)
+        rows = pl.ds(r, 32)
+        sent.append(pltpu.make_async_copy(held.at[rows, :], out_ref.at[rows, :], sems.at[r // 32]))
+        sent[-1].start()
+    for c in sent:
+        c.wait()
 
 
 def local(
@@ -628,7 +640,8 @@
         output_unit,
         out_shape=jax.ShapeDtypeStruct(tokens.shape, BF16),
         in_specs=[inner] * 5,
-        out_specs=inner,
+        out_specs=pl.BlockSpec(memory_space=pltpu.HBM),
+        scratch_shapes=[vm(tokens.shape, BF16), pltpu.SemaphoreType.DMA((4,))],
         compiler_params=pltpu.CompilerParams(vmem_limit_bytes=16000000),
         name="output_unit",
     )(response, glu_held, out_held, glu_bias.reshape(1, -1), out_gain.reshape(1, -1))

time: 26 us -> 25.5 us (0.981)
  Pallas kernels: 25.4 us -> 25.1 us
    pallas_call x1, Pallas kernels: 23.2 us -> 22.9 us  [local(): pl.pallas_call(kernel, out_shape=(vm((4, ROWS, 256), F32), vm(glu_weight....]
where the time goes in v5:
time: 25.5 us; the launch traced here: 25.1 us
  Pallas kernels  25.1 us (98%)
    pallas_call x1, Pallas kernels, local(): pl.pallas_call(kernel, out_shape=(vm((4, ROWS, 256), F32), vm(glu_weight....  22.9 us
    pallas_call x1, Pallas kernels, local(): pl.pallas_call(output_unit, out_shape=jax.ShapeDtypeStruct(tokens.shape,...  2.2 us

profile of v5, /device:TPU:1, one launch (start us, length us, event | category | flops | bytes accessed | tf_op | source)
XLA Modules:
  0.0 25.1 jit_solution(13599015171140245095)
XLA Ops:
  0.0 0.0 copy-start
  0.0 0.0 copy-start.1
  0.0 22.9 %ssm_layer.1 = (f32[4,128,256]{2,1,0:T(8,128)S(1)}, bf16[1024,1024]{1,0:T(8,128)(2,1)S(1)}, bf16[1024,2048]{1,0:T(8,128)(2,1)S(1)}) custom-call(bf16[128,2048]{1,0:T(8,128)(2,1)} %tokens_h.1, f32[1,128]{1,0:T(1,128)} %bitcast.11, f32[1,2048]{1,0:T(1,128)} %bitcast.9, bf16[2048,1024]{1,0:T(8,128)(2,1)} %inw_h.1, bf16[2,2,64,16,64]{4,3,2,1,0:T(8,128)(2,1)} %bitcast.8, ...), custom_call_target="tpu_custom_call" | custom-call | tf_op jit(solution)/shard_map/ssm_layer/pallas_call | solution.py:624
  22.9 0.0 copy-done
  22.9 0.0 copy-done.1
  22.9 2.2 %output_unit.1 = bf16[128,2048]{1,0:T(8,128)(2,1)} custom-call(f32[4,128,256]{2,1,0:T(8,128)S(1)} %get-tuple-element.8.resp, bf16[1024,1024]{1,0:T(8,128)(2,1)S(1)} %get-tuple-element.9.glu_v, bf16[1024,2048]{1,0:T(8,128)(2,1)S(1)} %get-tuple-element.10.outw_v, f32[1,1024]{1,0:T(1,128)S(1)} %bitcast.7, f32[1,2048]{1,0:T(1,128)S(1)} %bitcast.6), custom_call_target="tpu_custom_call" | custom-call | tf_op jit(solution)/shard_map/output_unit/pallas_call | solution.py:639
Async XLA Ops:
  0.0 22.9 %copy-start = (f32[2048]{0:T(1024)S(1)}, f32[2048]{0:T(1024)}, u32[]{:S(2)}) copy-start(f32[2048]{0:T(1024)} %param.25) | copy-start | bytes 24580
  0.0 22.9 %copy-start.1 = (f32[1024]{0:T(1024)S(1)}, f32[1024]{0:T(1024)}, u32[]{:S(2)}) copy-start(f32[1024]{0:T(1024)} %param.23) | copy-start | bytes 12292
